TPU v7x, 32 devices: a whole 2x2x4 slice. The times are simulated.
32 devices in a mesh: sp: 8 (over z, x), tp: 4 (over y, core).
Axes of the slice: x: 2, y: 2, z: 4, core: 2. Of those that a mesh axis runs over, the one named last changes fastest.
Arguments:
- tokens: bfloat16 [2048, 2048], P('sp'), may hold values from -6 to 6
- documents: int32 [2048], P('sp'), may hold values from 0 to 3, never falling along the last dimension, each value on 1 to 1024 neighbouring positions
- norm_gain: float32 [1, 2048], replicated, may hold values from 0.1 to 1.9
- w_query: bfloat16 [1, 2048, 2048], P(None, 'sp', 'tp'), may hold values from -0.125 to 0.125
- w_key: bfloat16 [1, 2048, 2048], P(None, 'sp', 'tp'), may hold values from -0.125 to 0.125
- w_value: bfloat16 [1, 2048, 2048], P(None, 'sp', 'tp'), may hold values from -0.125 to 0.125
- w_out: bfloat16 [1, 2048, 2048], P(None, None, 'sp'), may hold values from -0.59765625 to 0.59765625
- rel_bias: float32 [1, 32, 257], P(None, 'tp'), may hold values from -8 to 240
Outputs:
- mixed: bfloat16 [2048, 2048], P('sp')
Inputs may be any that keep to these rules, and one draw needn't show every extreme that they name: `documents`: document numbers never fall along the sequence; a document has 1 to 1024 positions.
All inputs are finite; a program needn't handle non-finite values.
Results may differ from a plain program's by a relative error of at most 0.007.
Values may be sent and summed in bfloat16 or wider, within the bound.
A program may use at most 128 MiB of HBM per device.

v0:
```python
import functools

import jax
import jax.numpy as jnp
from jax import lax
from jax.experimental import pallas as pl
from jax.experimental.pallas import tpu as pltpu
from jax.sharding import PartitionSpec as P

HEAD_DIM = 64
SEG = 64
LEFT = 4
REL_CLIP = 128


EPS = 1e-06


def passed_along(x, axis, by):
    length = lax.axis_size(axis)
    pairs = [(i, i + by) for i in range(length) if 0 <= i + by < length]
    return lax.ppermute(x, axis, pairs)


def banded_bias(bias_table, query_rows, key_rows, reach_rows):
    span_len = query_rows + key_rows - 1
    steps_back = jnp.arange(span_len, dtype=jnp.int32) - (key_rows - 1) + reach_rows
    lookup = jnp.clip(steps_back, -REL_CLIP, REL_CLIP) + REL_CLIP
    bias_line = jnp.take(bias_table, lookup, axis=1)
    reversed_line = bias_line[:, ::-1]
    repeated = jnp.tile(reversed_line, (1, query_rows))
    skewed = repeated[:, query_rows - 1 : query_rows - 1 + query_rows * (span_len - 1)]
    skewed = skewed.reshape(bias_table.shape[0], query_rows, span_len - 1)
    return skewed[:, :, :key_rows]


def attend(queries, keys_all, values_all, query_pos, key_pos, query_doc, key_doc, bias_table):
    query_rows = queries.shape[0]
    key_rows = keys_all.shape[0]
    reach_rows = key_rows - query_rows
    scores = jnp.einsum(
        "qhe,khe->hqk", queries, keys_all, preferred_element_type=jnp.float32
    ) * HEAD_DIM ** (-0.5)
    scores = scores + banded_bias(bias_table, query_rows, key_rows, reach_rows)
    query_seg = query_pos // SEG
    key_seg = key_pos // SEG
    allowed = (
        (key_pos[None, :] >= 0)
        & (key_seg[None, :] <= query_seg[:, None])
        & (key_seg[None, :] >= query_seg[:, None] - LEFT)
        & (key_doc[None, :] == query_doc[:, None])
    )
    scores = jnp.where(allowed[None], scores, -1e30)
    peak = jnp.max(scores, axis=-1, keepdims=True)
    raised = jnp.exp(scores - peak)
    weights_bf = (raised / jnp.sum(raised, axis=-1, keepdims=True)).astype(jnp.bfloat16)
    return jnp.einsum(
        "hqk,khe->qhe", weights_bf, values_all, preferred_element_type=jnp.float32
    ).astype(jnp.bfloat16)


def body(tokens, documents, norm_gain, w_query, w_key, w_value, w_out, rel_bias):
    local_rows = tokens.shape[0]
    reach_rows = LEFT * SEG
    width_local = w_query.shape[2]
    heads_local = width_local // HEAD_DIM
    offset = lax.axis_index("sp") * local_rows
    query_pos = offset + jnp.arange(local_rows, dtype=jnp.int32)
    key_pos = offset - reach_rows + jnp.arange(reach_rows + local_rows, dtype=jnp.int32)
    widened = tokens.astype(jnp.float32)
    normed = (
        widened
        * lax.rsqrt(jnp.mean(widened * widened, axis=-1, keepdims=True) + EPS)
        * norm_gain[0]
    ).astype(jnp.bfloat16)
    query_sum = jnp.dot(
        normed,
        lax.all_gather(w_query[0], "sp", axis=0, tiled=True),
        preferred_element_type=jnp.float32,
    )
    key_sum = jnp.dot(
        normed,
        lax.all_gather(w_key[0], "sp", axis=0, tiled=True),
        preferred_element_type=jnp.float32,
    )
    value_sum = jnp.dot(
        normed,
        lax.all_gather(w_value[0], "sp", axis=0, tiled=True),
        preferred_element_type=jnp.float32,
    )
    queries = query_sum.astype(jnp.bfloat16)
    keys_own = key_sum.astype(jnp.bfloat16)
    values_own = value_sum.astype(jnp.bfloat16)
    prior_keys, prior_values, prior_docs = passed_along((keys_own, values_own, documents), "sp", 1)
    keys_all = jnp.concatenate([prior_keys, keys_own], axis=0)
    values_all = jnp.concatenate([prior_values, values_own], axis=0)
    key_doc = jnp.concatenate([prior_docs, documents], axis=0)
    attended = attend(
        queries.reshape(local_rows, heads_local, HEAD_DIM),
        keys_all.reshape(reach_rows + local_rows, heads_local, HEAD_DIM),
        values_all.reshape(reach_rows + local_rows, heads_local, HEAD_DIM),
        query_pos,
        key_pos,
        documents,
        key_doc,
        rel_bias[0],
    ).reshape(local_rows, width_local)
    all_heads = lax.all_gather(attended, "tp", axis=1, tiled=True)
    return (
        widened
        + jnp.dot(
            all_heads,
            lax.all_gather(w_out[0], "sp", axis=1, tiled=True),
            preferred_element_type=jnp.float32,
        )
    ).astype(jnp.bfloat16)


MESH = pl.DeviceIdType.MESH
KEY, VALUE, QUERY, OUT = range(4)
UP, DOWN, ACROSS = range(3)
NEG = -1e30


def layer_kernel(
    n_sp, n_tp, doc_col, doc_row, gain_ref, line_ref, x_in, wk_in, wv_in, wq_in, wo_in, out_ref,
    w_all, w_mate, wo_all, x_ref, x_mate, normed, bias, q_buf, k_all, v_all, docs_all, docs_col, att, att_mate, done,
    own_sem, out_sem, mate_sem, x_sem, send_sem, recv_sem, swap_send, swap_recv, halo_send, halo_recv,
    tp_send, tp_recv, store_sem,
):
    rows, width = x_ref.shape
    depth, cols = wk_in.shape
    half_cols = cols // 2
    chunk = width // n_tp
    lanes = 2 * HEAD_DIM
    nz = n_sp // 2
    s = lax.axis_index("sp")
    t = lax.axis_index("tp")
    z, x = s // 2, s % 2
    mate = s + 1 - 2 * x
    ty, tc = t // 2, t % 2
    t_core = t + 1 - 2 * tc
    t_y = (1 - ty) * 2 + tc
    own_in = (wk_in, wv_in, wq_in)

    def slot(kind, block):
        if kind == OUT:
            return wo_all.at[block]
        return w_all.at[kind, pl.ds(pl.multiple_of(block * depth, depth), depth), :]

    def column_half(kind, which):
        return own_in[kind].at[:, pl.ds(pl.multiple_of(which * half_cols, half_cols), half_cols)]

    def own_copy(kind):
        return pltpu.make_async_copy(column_half(kind, x), slot(kind, s), own_sem.at[kind])

    def out_copy(r):
        return pltpu.make_async_copy(wo_in.at[pl.ds(r * cols, cols), :], slot(OUT, 2 * r + x), out_sem.at[r])

    def mate_copy(kind):
        return pltpu.make_async_copy(column_half(kind, 1 - x), w_mate.at[kind], mate_sem.at[kind])

    x_copy = pltpu.make_async_copy(x_in, x_ref, x_sem)
    for kind in range(3):
        own_copy(kind).start()
        mate_copy(kind).start()
    x_copy.start()

    @pl.when(z == t)
    def _():
        for r in range(n_tp):
            out_copy(r).start()


    def move(way, kind, block):
        target = (s + 2, s - 2, mate)[way]
        src = slot(kind, block)
        if way == ACROSS and kind != OUT:
            src = w_mate.at[kind]
        return pltpu.make_async_remote_copy(
            src_ref=src, dst_ref=slot(kind, block),
            send_sem=send_sem.at[way, kind, block], recv_sem=recv_sem.at[kind, block],
            device_id={"sp": target}, device_id_type=MESH,
        )

    def halo(i):
        buf = (k_all, v_all, docs_all)[i]
        if i == 2:
            src, dst = buf.at[:, pl.ds(2 * rows, rows)], buf.at[:, pl.ds(0, rows)]
        else:
            src, dst = buf.at[pl.ds(2 * rows, rows), :], buf.at[pl.ds(0, rows), :]
        return pltpu.make_async_remote_copy(
            src_ref=src, dst_ref=dst, send_sem=halo_send.at[i], recv_sem=halo_recv.at[i],
            device_id={"sp": s + 2}, device_id_type=MESH,
        )

    def block_of(which):
        return pl.ds(pl.multiple_of(which * rows, rows), rows)

    def swap(i, src, dst):
        return pltpu.make_async_remote_copy(
            src_ref=src, dst_ref=dst, send_sem=swap_send.at[i], recv_sem=swap_recv.at[i],
            device_id={"sp": mate}, device_id_type=MESH,
        )

    x_swap = swap(0, x_ref, x_mate)
    row_swap = swap(1, doc_row, docs_all.at[:, block_of(1 + x)])
    col_swap = swap(2, doc_col, docs_col.at[block_of(x), :])
    att_half = pl.ds(pl.multiple_of(x * half_cols, half_cols), half_cols)
    att_swap = swap(3, att_mate, att.at[t, :, att_half])

    has_up, has_down = z < nz - 1, z > 0

    barrier = pltpu.get_barrier_semaphore()
    for peer in (mate, lax.rem(s + 2, n_sp), lax.rem(s + n_sp - 2, n_sp)):
        pl.semaphore_signal(barrier, inc=1, device_id={"sp": peer}, device_id_type=MESH)
    for peer in (t_core, t_y):
        pl.semaphore_signal(barrier, inc=1, device_id={"tp": peer}, device_id_type=MESH)
    pl.semaphore_wait(barrier, 5)

    def along_z(kind, block):
        pl.when(has_up)(lambda: move(UP, kind, block).start())
        pl.when(has_down)(lambda: move(DOWN, kind, block).start())

    def send_own(kind):
        own_copy(kind).wait()
        along_z(kind, s)

    def send_mate(kind):
        mate_copy(kind).wait()
        move(ACROSS, kind, s).start()

    def forward_mate(kind):
        move(ACROSS, kind, mate).wait_recv()
        along_z(kind, mate)

    def forward(kind, d):
        for start in (s, mate):
            @pl.when(z - d >= 0)
            def _():
                block = start - 2 * d
                move(UP, kind, block).wait_recv()
                pl.when(has_up)(lambda: move(UP, kind, block).start())

            @pl.when(z + d < nz)
            def _():
                block = start + 2 * d
                move(DOWN, kind, block).wait_recv()
                pl.when(has_down)(lambda: move(DOWN, kind, block).start())

    sends_up, sends_down = (z >= t) & has_up, (z <= t) & has_down

    def send_out(r):
        pl.when(sends_up)(lambda: move(UP, OUT, 2 * r + x).start())
        pl.when(sends_down)(lambda: move(DOWN, OUT, 2 * r + x).start())
        move(ACROSS, OUT, 2 * r + x).start()

    def forward_out(r):
        @pl.when(z != t)
        def _():
            move(UP, OUT, 2 * r + x).wait_recv()
            send_out(r)

    def normalize(src, which):
        wide = src[...].astype(jnp.float32)
        normed[block_of(which), :] = (
            wide * lax.rsqrt(jnp.mean(wide * wide, axis=-1, keepdims=True) + EPS) * gain_ref[...]
        ).astype(jnp.bfloat16)

    send_mate(KEY)
    send_own(KEY)
    send_mate(VALUE)
    send_own(VALUE)
    send_mate(QUERY)
    x_copy.wait()
    x_swap.start()
    row_swap.start()
    col_swap.start()

    docs_all[:, block_of(1 + x)] = doc_row[...]
    docs_col[block_of(x), :] = doc_col[...]

    @pl.when(z == 0)
    def _():
        docs_all[:, pl.ds(0, rows)] = jnp.full((8, rows), -1, jnp.int32)
        k_all[pl.ds(0, rows), :] = jnp.zeros((rows, half_cols), jnp.bfloat16)
        v_all[pl.ds(0, rows), :] = jnp.zeros((rows, half_cols), jnp.bfloat16)

    forward_mate(KEY)
    normalize(x_ref, x)
    forward(KEY, 1)

    q_rows, span = 2 * SEG, (LEFT + 2) * SEG
    heads = half_cols // HEAD_DIM
    q_seg = lax.broadcasted_iota(jnp.int32, (q_rows, span), 0) // SEG
    k_seg = lax.broadcasted_iota(jnp.int32, (q_rows, span), 1) // SEG
    near = (k_seg >= q_seg) & (k_seg <= q_seg + LEFT)
    for h in range(heads):
        line = jnp.broadcast_to(line_ref[pl.ds(x * heads + h, 1), :], (q_rows, line_ref.shape[1]))
        skew = pltpu.roll(line, 0, 1, stride=1, stride_axis=0)
        bias[h] = jnp.where(near, skew[:, :span], NEG)

    def project(kind):
        return jnp.dot(normed[...], w_all[kind], preferred_element_type=jnp.float32)

    forward_mate(VALUE)
    for d in range(2, nz):
        forward(KEY, d)
    send_own(QUERY)
    forward_mate(QUERY)
    for d in range(1, nz):
        forward(VALUE, d)
    x_swap.wait_recv()
    normalize(x_mate, 1 - x)
    k_all[pl.ds(rows, 2 * rows), :] = project(KEY).astype(jnp.bfloat16)
    row_swap.wait_recv()
    col_swap.wait_recv()
    forward(QUERY, 1)
    pl.when(has_up)(lambda: halo(0).start())
    pl.when(has_up)(lambda: halo(2).start())
    v_all[pl.ds(rows, 2 * rows), :] = project(VALUE).astype(jnp.bfloat16)
    for d in range(2, nz - 1):
        forward(QUERY, d)
    pl.when(has_up)(lambda: halo(1).start())

    @pl.when(z == t)
    def _():
        for r in range(n_tp):
            out_copy(r).wait()
            send_out(r)

    forward(QUERY, nz - 1)
    q_buf[...] = (project(QUERY).astype(jnp.bfloat16).astype(jnp.float32) * HEAD_DIM ** (-0.5)).astype(jnp.bfloat16)

    @pl.when(has_down)
    def _():
        for i in range(3):
            halo(i).wait_recv()

    low = lax.broadcasted_iota(jnp.int32, (q_rows, lanes), 1) < HEAD_DIM

    def attend_rows(which, j):
        first = pl.multiple_of(which * rows + j * q_rows, q_rows)
        queries, keys = pl.ds(first, q_rows), pl.ds(first, span)
        same = docs_col[queries, :][:, :1] == docs_all[pl.ds(0, 1), keys]
        found = []
        for p in range(half_cols // lanes):
            q_pair = q_buf[queries, pl.ds(p * lanes, lanes)]
            k_pair = k_all[keys, pl.ds(p * lanes, lanes)]
            v_pair = v_all[keys, pl.ds(p * lanes, lanes)]
            both = []
            for half in range(2):
                mine = low if half == 0 else jnp.logical_not(low)
                q_one = jnp.where(mine, q_pair, jnp.zeros_like(q_pair))
                score = lax.dot_general(
                    q_one, k_pair, (((1,), (1,)), ((), ())), preferred_element_type=jnp.float32
                )
                score = jnp.where(same, score + bias[2 * p + half], NEG)
                raised = jnp.exp(score - jnp.max(score, axis=-1, keepdims=True))
                total = jnp.sum(raised, axis=-1, keepdims=True)
                both.append(
                    jnp.dot(raised.astype(jnp.bfloat16), v_pair, preferred_element_type=jnp.float32) / total
                )
            found.append(jnp.where(low, both[0], both[1]).astype(jnp.bfloat16))
        return jnp.concatenate(found, axis=1)

    def tp_move(i, ref, which, target):
        return pltpu.make_async_remote_copy(
            src_ref=ref.at[which], dst_ref=ref.at[which], send_sem=tp_send.at[i], recv_sem=tp_recv.at[i],
            device_id={"tp": target}, device_id_type=MESH,
        )

    att_y = tp_move(0, att, t, t_y)
    att_core = tp_move(1, att, t, t_core)
    att_on = tp_move(2, att, t_y, t_core)

    parts = rows // q_rows
    for j in range(parts):
        att_mate[pl.ds(j * q_rows, q_rows), :] = attend_rows(1 - x, j)
    forward_out(0)
    for j in range(parts):
        att[t, pl.ds(j * q_rows, q_rows), att_half] = attend_rows(x, j)
        if j == 0:
            att_swap.start()
    forward_out(1)
    att_swap.wait_recv()
    att_y.start()
    att_core.start()
    for r in range(2, n_tp):
        forward_out(r)
    att_y.wait_recv()
    att_on.start()
    att_core.wait_recv()
    att_on.wait_recv()
    for r in range(n_tp):
        move(ACROSS, OUT, 2 * r + 1 - x).wait_recv()
    sums = [x_ref[:, pl.ds(pl.multiple_of(t * chunk + i * (chunk // 2), chunk // 2), chunk // 2)].astype(jnp.float32) for i in range(2)]
    for i in range(2):
        made = jnp.zeros_like(sums[i])
        for r in range(n_tp):
            made = made + jnp.dot(att[r], wo_all[2 * r + i], preferred_element_type=jnp.float32)
        done[t, :, pl.ds(i * (chunk // 2), chunk // 2)] = (sums[i] + made).astype(jnp.bfloat16)

    def store(which):
        return pltpu.make_async_copy(
            done.at[which], out_ref.at[:, pl.ds(pl.multiple_of(which * chunk, chunk), chunk)], store_sem.at[which]
        )

    far_core = (1 - ty) * 2 + (1 - tc)
    to_y = tp_move(3, done, t, t_y)
    to_core = tp_move(4, done, t, t_core)
    pass_on = tp_move(5, done, t_y, t_core)
    to_y.start()
    to_core.start()
    store(t).start()
    to_y.wait_recv()
    pass_on.start()
    store(t_y).start()
    to_core.wait_recv()
    store(t_core).start()
    pass_on.wait_recv()
    store(far_core).start()
    for which in range(n_tp):
        store(which).wait()

    for kind in range(3):
        move(ACROSS, kind, s).wait_send()
        for start in (s, mate):
            for d in range(nz):
                @pl.when(z - d >= 0)
                def _():
                    pl.when(has_up)(lambda: move(UP, kind, start - 2 * d).wait_send())

                @pl.when(z + d < nz)
                def _():
                    pl.when(has_down)(lambda: move(DOWN, kind, start + 2 * d).wait_send())
    for r in range(n_tp):
        pl.when(sends_up)(lambda: move(UP, OUT, 2 * r + x).wait_send())
        pl.when(sends_down)(lambda: move(DOWN, OUT, 2 * r + x).wait_send())
        move(ACROSS, OUT, 2 * r + x).wait_send()

    @pl.when(has_up)
    def _():
        for i in range(3):
            halo(i).wait_send()
    for one in (x_swap, row_swap, col_swap, att_swap, att_y, att_core, att_on, to_y, to_core, pass_on):
        one.wait_send()


def body_one(n_sp, n_tp, tokens, documents, norm_gain, w_query, w_key, w_value, w_out, rel_bias):
    rows, width = tokens.shape
    depth, cols = w_query.shape[1:]
    heads = cols // HEAD_DIM
    out_cols = w_out.shape[2]
    chunk = width // n_tp
    reach = LEFT * SEG
    table = rel_bias[0]
    furthest = table[:, 2 * REL_CLIP:]
    ahead, behind = reach - REL_CLIP, reach - REL_CLIP - 1
    line = jnp.concatenate(
        [
            jnp.broadcast_to(furthest, (heads, ahead)),
            table[:, ::-1],
            jnp.broadcast_to(furthest, (heads, behind)),
        ],
        axis=1,
    )
    doc_col = jnp.broadcast_to(documents[:, None], (rows, 128))
    doc_row = jnp.broadcast_to(documents[None, :], (8, rows))
    bf, f32 = jnp.bfloat16, jnp.float32
    vmem = pl.BlockSpec(memory_space=pltpu.VMEM)
    hbm = pl.BlockSpec(memory_space=pl.ANY)
    dma = pltpu.SemaphoreType.DMA
    return pl.pallas_call(
        functools.partial(layer_kernel, n_sp, n_tp),
        out_shape=jax.ShapeDtypeStruct((rows, width), bf),
        in_specs=[vmem] * 4 + [hbm] * 5,
        out_specs=hbm,
        scratch_shapes=[
            pltpu.VMEM((3, n_sp * depth, cols // 2), bf),
            pltpu.VMEM((3, depth, cols // 2), bf),
            pltpu.VMEM((n_sp, cols, out_cols), bf),
            pltpu.VMEM((rows, width), bf),
            pltpu.VMEM((rows, width), bf),
            pltpu.VMEM((2 * rows, width), bf),
            pltpu.VMEM((heads // 2, 2 * SEG, (LEFT + 2) * SEG), f32),
            pltpu.VMEM((2 * rows, cols // 2), bf),
            pltpu.VMEM((3 * rows, cols // 2), bf),
            pltpu.VMEM((3 * rows, cols // 2), bf),
            pltpu.VMEM((8, 3 * rows), jnp.int32),
            pltpu.VMEM((2 * rows, 128), jnp.int32),
            pltpu.VMEM((n_tp, rows, cols), bf),
            pltpu.VMEM((rows, cols // 2), bf),
            pltpu.VMEM((n_tp, rows, chunk), bf),
            dma((3,)),
            dma((n_tp,)),
            dma((3,)),
            dma(()),
            dma((3, 4, n_sp)),
            dma((4, n_sp)),
            dma((4,)),
            dma((4,)),
            dma((3,)),
            dma((3,)),
            dma((6,)),
            dma((6,)),
            dma((n_tp,)),
        ],
        compiler_params=pltpu.CompilerParams(
            collective_id=0, has_side_effects=True, vmem_limit_bytes=60 * 1024 * 1024
        ),
    )(doc_col, doc_row, norm_gain, line, tokens, w_key[0], w_value[0], w_query[0], w_out[0])


def fits_one(mesh):
    return mesh.shape["tp"] == 4 and mesh.shape["sp"] == 2 * mesh.shape["tp"]


def solution(mesh):
    n_sp, n_tp = mesh.shape["sp"], mesh.shape["tp"]
    run = functools.partial(body_one, n_sp, n_tp) if fits_one(mesh) else body
    in_specs = (
        P("sp", None),
        P("sp"),
        P(),
        P(None, "sp", "tp"),
        P(None, "sp", "tp"),
        P(None, "sp", "tp"),
        P(None, None, "sp"),
        P(None, "tp", None),
    )
    out_specs = P("sp", None)
    return jax.shard_map(run, mesh=mesh, in_specs=in_specs, out_specs=out_specs, check_vma=False)
```

profile of v0, /device:TPU:0, one launch (start us, length us, event | category | flops | bytes accessed | tf_op | source)
XLA Modules:
  0.0 109.1 jit_solution(17753866843530289334)
XLA Ops:
  0.0 0.0 copy-start
  0.0 0.9 slice_reduce_fusion
  0.9 0.1 broadcast_in_dim.28
  0.9 0.0 copy-start.1
  0.9 0.1 broadcast_in_dim.13
  1.0 0.6 copy-done.1
  1.6 0.6 broadcast_in_dim.11.doc_row
  2.2 0.0 copy-done
  2.2 0.2 reverse
  2.4 0.1 slice.6
  2.5 0.7 pad_maximum_fusion.line_ref
  3.2 0.8 broadcast_in_dim.10.doc_col
  4.0 102.8 %shard_map.82 = bf16[256,2048]{1,0:T(8,128)(2,1)} custom-call(s32[256,128]{1,0:T(8,128)} %broadcast_in_dim.10.doc_col, s32[8,256]{1,0:T(8,128)} %broadcast_in_dim.11.doc_row, f32[1,2048]{1,0:T(1,128)} %gain_ref.1, f32[8,512]{1,0:T(8,128)} %pad_maximum_fusion.line_ref, bf16[256,2048]{1,0:T(8,128)(2,1)} %x_in.1, bf16[256,512]{1,0:T(8,128)(2,1)} %bitcast.7, ...), custom_call_target="tpu_custom_call" | custom-call | tf_op jit(solution)/shard_map/pallas_call | solution.py:474
  106.8 2.3 %copy.10 = bf16[256,2048]{1,0:T(8,128)(2,1)} copy(bf16[256,2048]{1,0:T(8,128)(2,1)} %shard_map.82) | data formatting | bytes 2097152
Async XLA Ops:
  0.0 2.2 %copy-start = (f32[1,8,257]{2,1,0:T(8,128)S(1)}, f32[1,8,257]{2,1,0:T(8,128)}, u32[]{:S(2)}) copy-start(f32[1,8,257]{2,1,0:T(8,128)} %param.15) | copy-start | bytes 24676
  0.9 0.7 copy-start.1
where the time goes:
time: 109 us
  Pallas kernels  103 us (94%)
  local copies, waits for them, and re-layouts  5.57 us (5%)
    pallas_call x1, Pallas kernels, body_one(): pl.pallas_call(functools.partial(layer_kernel, n_sp, n_tp), out_shape=jax...  103 us
    unnamed x7, local copies, waits for them, and re-layouts  3.21 us

commit v1 on v0

v1 whole, which is shorter than its diff:
```python
import functools

import jax
import jax.numpy as jnp
from jax import lax
from jax.experimental import pallas as pl
from jax.experimental.pallas import tpu as pltpu
from jax.sharding import PartitionSpec as P

HEAD_DIM = 64
SEG = 64
LEFT = 4
REL_CLIP = 128


EPS = 1e-06


def passed_along(x, axis, by):
    length = lax.axis_size(axis)
    pairs = [(i, i + by) for i in range(length) if 0 <= i + by < length]
    return lax.ppermute(x, axis, pairs)


def banded_bias(bias_table, query_rows, key_rows, reach_rows):
    span_len = query_rows + key_rows - 1
    steps_back = jnp.arange(span_len, dtype=jnp.int32) - (key_rows - 1) + reach_rows
    lookup = jnp.clip(steps_back, -REL_CLIP, REL_CLIP) + REL_CLIP
    bias_line = jnp.take(bias_table, lookup, axis=1)
    reversed_line = bias_line[:, ::-1]
    repeated = jnp.tile(reversed_line, (1, query_rows))
    skewed = repeated[:, query_rows - 1 : query_rows - 1 + query_rows * (span_len - 1)]
    skewed = skewed.reshape(bias_table.shape[0], query_rows, span_len - 1)
    return skewed[:, :, :key_rows]


def attend(queries, keys_all, values_all, query_pos, key_pos, query_doc, key_doc, bias_table):
    query_rows = queries.shape[0]
    key_rows = keys_all.shape[0]
    reach_rows = key_rows - query_rows
    scores = jnp.einsum(
        "qhe,khe->hqk", queries, keys_all, preferred_element_type=jnp.float32
    ) * HEAD_DIM ** (-0.5)
    scores = scores + banded_bias(bias_table, query_rows, key_rows, reach_rows)
    query_seg = query_pos // SEG
    key_seg = key_pos // SEG
    allowed = (
        (key_pos[None, :] >= 0)
        & (key_seg[None, :] <= query_seg[:, None])
        & (key_seg[None, :] >= query_seg[:, None] - LEFT)
        & (key_doc[None, :] == query_doc[:, None])
    )
    scores = jnp.where(allowed[None], scores, -1e30)
    peak = jnp.max(scores, axis=-1, keepdims=True)
    raised = jnp.exp(scores - peak)
    weights_bf = (raised / jnp.sum(raised, axis=-1, keepdims=True)).astype(jnp.bfloat16)
    return jnp.einsum(
        "hqk,khe->qhe", weights_bf, values_all, preferred_element_type=jnp.float32
    ).astype(jnp.bfloat16)


def body(tokens, documents, norm_gain, w_query, w_key, w_value, w_out, rel_bias):
    local_rows = tokens.shape[0]
    reach_rows = LEFT * SEG
    width_local = w_query.shape[2]
    heads_local = width_local // HEAD_DIM
    offset = lax.axis_index("sp") * local_rows
    query_pos = offset + jnp.arange(local_rows, dtype=jnp.int32)
    key_pos = offset - reach_rows + jnp.arange(reach_rows + local_rows, dtype=jnp.int32)
    widened = tokens.astype(jnp.float32)
    normed = (
        widened
        * lax.rsqrt(jnp.mean(widened * widened, axis=-1, keepdims=True) + EPS)
        * norm_gain[0]
    ).astype(jnp.bfloat16)
    query_sum = jnp.dot(
        normed,
        lax.all_gather(w_query[0], "sp", axis=0, tiled=True),
        preferred_element_type=jnp.float32,
    )
    key_sum = jnp.dot(
        normed,
        lax.all_gather(w_key[0], "sp", axis=0, tiled=True),
        preferred_element_type=jnp.float32,
    )
    value_sum = jnp.dot(
        normed,
        lax.all_gather(w_value[0], "sp", axis=0, tiled=True),
        preferred_element_type=jnp.float32,
    )
    queries = query_sum.astype(jnp.bfloat16)
    keys_own = key_sum.astype(jnp.bfloat16)
    values_own = value_sum.astype(jnp.bfloat16)
    prior_keys, prior_values, prior_docs = passed_along((keys_own, values_own, documents), "sp", 1)
    keys_all = jnp.concatenate([prior_keys, keys_own], axis=0)
    values_all = jnp.concatenate([prior_values, values_own], axis=0)
    key_doc = jnp.concatenate([prior_docs, documents], axis=0)
    attended = attend(
        queries.reshape(local_rows, heads_local, HEAD_DIM),
        keys_all.reshape(reach_rows + local_rows, heads_local, HEAD_DIM),
        values_all.reshape(reach_rows + local_rows, heads_local, HEAD_DIM),
        query_pos,
        key_pos,
        documents,
        key_doc,
        rel_bias[0],
    ).reshape(local_rows, width_local)
    all_heads = lax.all_gather(attended, "tp", axis=1, tiled=True)
    return (
        widened
        + jnp.dot(
            all_heads,
            lax.all_gather(w_out[0], "sp", axis=1, tiled=True),
            preferred_element_type=jnp.float32,
        )
    ).astype(jnp.bfloat16)


MESH = pl.DeviceIdType.MESH
TOK, OUT = range(2)
UP, DOWN, ACROSS = range(3)
W0, W1, A0, A1 = range(4)
NEG = -1e30


def plane_of(t):
    c = t % 2
    return 3 * c + (t // 2) * (1 - 2 * c)


def part_for(z):
    return 2 * (((z + 1) // 2) % 2) + z // 2


def layer_kernel(
    n_sp, n_tp, doc_row, gain_ref, line_ref, x_in, wk_in, wv_in, wq_in, wo_in, out_ref,
    w_own, w_relay, w_all, wo_all, tok, resid, normed, line_all, bias, q_buf, kv_all, docs_all, mask,
    att_own, att_relay, att_all, done,
    own_sem, loc_sem, out_sem, tok_sem, res_sem, line_send, line_recv, hop_send, relay_recv, rep_send, rep_recv,
    cast_send, cast_recv, halo_send, halo_recv, tp_send, tp_recv, store_sem,
):
    rows, width = tok.shape[1:]
    depth, cols = wk_in.shape
    half_cols = cols // 2
    lanes = 2 * HEAD_DIM
    pairs = half_cols // lanes
    chunk = width // n_tp
    nz = n_sp // 2
    pieces = n_tp
    piece = rows // pieces
    s = lax.axis_index("sp")
    t = lax.axis_index("tp")
    z, x = s // 2, s % 2
    mate = s + 1 - 2 * x
    ty, tc = t // 2, t % 2
    t_core = t + 1 - 2 * tc
    t_y = (1 - ty) * 2 + tc
    t_far = (1 - ty) * 2 + 1 - tc
    home, home_y = plane_of(t), plane_of(t_y)
    first_entry, second_entry = z == home, z == home_y
    entry = first_entry | second_entry
    gap = z - home
    is_first = 1 - (gap * gap + n_sp) // (n_sp + 1)
    x_mine = x * is_first + (1 - x) * (1 - is_first)
    own_in = (wk_in, wv_in, wq_in)
    has_up, has_down = z < nz - 1, z > 0

    def at_multiple(start, size, step):
        return pl.ds(pl.multiple_of(start, step), size)

    def weight_cols(which, p):
        return at_multiple(which * half_cols + p * lanes, lanes, lanes)

    def kind_cols(kind):
        return pl.ds(kind * lanes, lanes)

    def own_copy(i, p, kind):
        which = x if i == 0 else 1 - x
        return pltpu.make_async_copy(
            own_in[kind].at[:, weight_cols(which, p)], w_own.at[i, p, :, kind_cols(kind)], own_sem.at[i, p, kind]
        )

    def local_copy(p, kind):
        return pltpu.make_async_copy(
            own_in[kind].at[:, weight_cols(x, p)],
            w_all.at[p, at_multiple(s * depth, depth, depth), kind_cols(kind)], loc_sem.at[p, kind],
        )

    def tok_copy(r):
        part = pl.ds(r * piece, piece)
        return pltpu.make_async_copy(x_in.at[part, :], tok.at[x, part, :], tok_sem.at[r])

    def out_copy(r):
        return pltpu.make_async_copy(wo_in.at[pl.ds(r * cols, cols), :], wo_all.at[2 * r + x], out_sem.at[r])

    resid_copy = pltpu.make_async_copy(x_in.at[:, at_multiple(home_y * chunk, chunk, chunk)], resid, res_sem)

    @pl.when(first_entry)
    def _():
        for r in range(pieces):
            tok_copy(r).start()

    for p in range(pairs):
        for i in (1, 0):
            for kind in range(3):
                own_copy(i, p, kind).start()

    @pl.when(first_entry)
    def _():
        for p in range(pairs):
            for kind in range(3):
                local_copy(p, kind).start()

    @pl.when(second_entry)
    def _():
        for r in range(n_tp):
            out_copy(r).start()

    resid_copy.start()

    def remote(src, dst, send, recv, **where):
        return pltpu.make_async_remote_copy(
            src_ref=src, dst_ref=dst, send_sem=send, recv_sem=recv, device_id=where, device_id_type=MESH
        )

    def slot(ch, block):
        if ch < A0:
            return w_all.at[ch - W0, at_multiple(block * depth, depth, depth), :]
        start = (block % 2) * half_cols + (ch - A0) * lanes
        return att_all.at[part_for(block // 2), :, at_multiple(start, lanes, lanes)]

    def own_ref(ch, i):
        return w_own.at[i, ch - W0] if ch < A0 else att_own.at[ch - A0, x if i == 0 else 1 - x]

    def relay_ref(ch):
        return w_relay.at[ch - W0] if ch < A0 else att_relay.at[ch - A0]

    def direct(ch):
        return remote(own_ref(ch, 0), slot(ch, s), hop_send.at[ch, 0], rep_recv.at[ch, s], sp=2 * home + x)

    def cross_in(ch):
        return remote(own_ref(ch, 1), slot(ch, s), hop_send.at[ch, 1], rep_recv.at[ch, s], sp=mate, tp=t_y)

    def cross_relay(ch):
        return remote(own_ref(ch, 1), relay_ref(ch), hop_send.at[ch, 1], relay_recv.at[ch], sp=mate, tp=t_y)

    def relay(ch):
        return remote(relay_ref(ch), slot(ch, mate), hop_send.at[ch, 2], rep_recv.at[ch, mate], sp=2 * home_y + x)

    def to_y(ch, block):
        return remote(slot(ch, block), slot(ch, block), rep_send.at[ch, 0, block], rep_recv.at[ch, block], tp=t_y)

    def to_core(ch, block):
        return remote(slot(ch, block), slot(ch, block), rep_send.at[ch, 1, block], rep_recv.at[ch, block], tp=t_core)

    def send_cross(ch):
        pl.when(first_entry)(lambda: cross_in(ch).start())
        pl.when(jnp.logical_not(first_entry))(lambda: cross_relay(ch).start())

    def send_direct(ch):
        pl.when(jnp.logical_not(first_entry))(lambda: direct(ch).start())

    def send_relay(ch):
        @pl.when(jnp.logical_not(second_entry))
        def _():
            cross_relay(ch).wait_recv()
            relay(ch).start()

    planes = [0]
    for d in range(1, nz):
        planes += [-d, d]

    def valid(off):
        return (z + off >= 0) & (z + off < nz)

    def mine(ch, off):
        @pl.when(entry & valid(off))
        def _():
            block = 2 * (z + off) + x_mine
            if off == 0:
                pl.when(jnp.logical_not(first_entry))(lambda: to_y(ch, block).wait_recv())
                if ch < A0:
                    @pl.when(first_entry)
                    def _():
                        for kind in range(3):
                            local_copy(ch - W0, kind).wait()
            else:
                to_y(ch, block).wait_recv()
            to_y(ch, block).start()
            to_core(ch, block).start()

    def theirs(ch, off):
        @pl.when(valid(off))
        def _():
            @pl.when(entry)
            def _():
                block = 2 * (z + off) + 1 - x_mine
                to_y(ch, block).wait_recv()
                to_core(ch, block).start()

            @pl.when(jnp.logical_not(entry))
            def _():
                for i in range(2):
                    to_core(ch, 2 * (z + off) + i).wait_recv()

    def spread(ch, first, last):
        for i in range(first, last + 1):
            if i < len(planes):
                mine(ch, planes[i])
            if i > 0:
                theirs(ch, planes[i - 1])

    def drain(ch):
        pl.when(jnp.logical_not(first_entry))(lambda: direct(ch).wait_send())
        cross_relay(ch).wait_send()
        pl.when(jnp.logical_not(second_entry))(lambda: relay(ch).wait_send())

        @pl.when(entry)
        def _():
            for zz in range(nz):
                to_y(ch, 2 * zz + x_mine).wait_send()
                for i in range(2):
                    to_core(ch, 2 * zz + i).wait_send()

    def cast_ref(kind, which, r):
        if kind == OUT:
            return wo_all.at[2 * r + which]
        if r == pieces:
            return docs_all.at[:, at_multiple((1 + which) * rows, rows, rows)]
        return tok.at[which, pl.ds(r * piece, piece), :]

    def move(kind, way, r, src=None):
        ref = cast_ref(kind, x, r)
        return remote(
            ref if src is None else src, ref, cast_send.at[kind, way, r], cast_recv.at[kind, x, r],
            sp=(s + 2, s - 2, mate)[way],
        )

    def across_in(kind, r):
        ref = cast_ref(kind, 1 - x, r)
        return remote(ref, ref, cast_send.at[kind, ACROSS, r], cast_recv.at[kind, 1 - x, r], sp=mate)

    centers = (home, home_y)

    def cast_send_on(kind, r, src=None):
        pl.when((z >= centers[kind]) & has_up)(lambda: move(kind, UP, r, src).start())
        pl.when((z <= centers[kind]) & has_down)(lambda: move(kind, DOWN, r, src).start())
        move(kind, ACROSS, r, src).start()

    def cast_source(kind, r):
        if r == pieces and kind == TOK:
            docs_all[:, at_multiple((1 + x) * rows, rows, rows)] = doc_row[...]
            cast_send_on(kind, r, doc_row)
            return
        (tok_copy, out_copy)[kind](r).wait()
        cast_send_on(kind, r)

    def cast_forward(kind, r):
        @pl.when(z != centers[kind])
        def _():
            move(kind, UP, r).wait_recv()
            cast_send_on(kind, r)

    def cast_drain(kind, count):
        for r in range(count):
            pl.when((z >= centers[kind]) & has_up)(lambda: move(kind, UP, r).wait_send())
            pl.when((z <= centers[kind]) & has_down)(lambda: move(kind, DOWN, r).wait_send())
            move(kind, ACROSS, r).wait_send()

    line_targets = (t_core, t_y, t_far)

    def line_copy(i):
        return remote(line_ref, line_all, line_send.at[i], line_recv, tp=line_targets[i])

    has_next, has_prev = home < nz - 1, home > 0

    def halo(i):
        if i == pairs:
            src, dst = docs_all.at[:, pl.ds(2 * rows, rows)], docs_all.at[:, pl.ds(0, rows)]
        else:
            src, dst = kv_all.at[i, pl.ds(2 * rows, rows), :], kv_all.at[i, pl.ds(0, rows), :]
        return remote(src, dst, halo_send.at[i], halo_recv.at[i], tp=part_for((home + 1) % nz))

    barrier = pltpu.get_barrier_semaphore()
    for d in range(1, nz):
        pl.semaphore_signal(
            barrier, inc=1, device_id={"sp": lax.rem(s + 2 * d, n_sp)}, device_id_type=MESH
        )
    for peer in (t_core, t_y, t_far):
        pl.semaphore_signal(barrier, inc=1, device_id={"tp": peer}, device_id_type=MESH)
    for peer in (t, t_y):
        pl.semaphore_signal(barrier, inc=1, device_id={"sp": mate, "tp": peer}, device_id_type=MESH)
    pl.semaphore_wait(barrier, nz + 4)

    @pl.when(first_entry)
    def _():
        cast_source(TOK, pieces)
        cast_source(TOK, 0)

    for p in range(pairs):
        for i in (1, 0):
            for kind in range(3):
                own_copy(i, p, kind).wait()
            (send_direct, send_cross)[i](W0 + p)

    @pl.when(first_entry)
    def _():
        for r in range(1, pieces):
            cast_source(TOK, r)
        for i in range(3):
            line_copy(i).start()

    @pl.when(has_prev == False)
    def _():
        docs_all[:, pl.ds(0, rows)] = jnp.full((8, rows), -1, jnp.int32)
        for p in range(pairs):
            kv_all[p, pl.ds(0, rows), :] = jnp.zeros((rows, 2 * lanes), jnp.bfloat16)

    send_relay(W0)
    cast_forward(TOK, pieces)
    cast_forward(TOK, 0)
    send_relay(W1)
    spread(W0, 0, 0)
    cast_forward(TOK, 1)
    spread(W0, 1, 2)
    cast_forward(TOK, 2)
    spread(W0, 3, 4)
    cast_forward(TOK, 3)
    spread(W0, 5, 7)

    def normalize(which):
        wide = tok[which].astype(jnp.float32)
        normed[at_multiple(which * rows, rows, rows), :] = (
            wide * lax.rsqrt(jnp.mean(wide * wide, axis=-1, keepdims=True) + EPS) * gain_ref[...]
        ).astype(jnp.bfloat16)

    normalize(x)
    spread(W1, 0, 2)

    q_rows, span = 2 * SEG, (LEFT + 2) * SEG
    heads = half_cols // HEAD_DIM
    blocks = 2 * rows // q_rows

    pl.when(first_entry)(lambda: line_all.__setitem__(Ellipsis, line_ref[...]))
    pl.when(jnp.logical_not(first_entry))(lambda: line_copy(0).wait_recv())
    q_seg = lax.broadcasted_iota(jnp.int32, (q_rows, span), 0) // SEG
    k_seg = lax.broadcasted_iota(jnp.int32, (q_rows, span), 1) // SEG
    near = (k_seg >= q_seg) & (k_seg <= q_seg + LEFT)
    for h in range(heads):
        line = jnp.broadcast_to(line_all[pl.ds(x * heads + h, 1), :], (q_rows, line_ref.shape[1]))
        skew = pltpu.roll(line, 0, 1, stride=1, stride_axis=0)
        bias[h] = jnp.where(near, skew[:, :span], NEG)

    for r in range(pieces + 1):
        across_in(TOK, r).wait_recv()
    normalize(1 - x)
    pl.when(has_next)(lambda: halo(pairs).start())
    spread(W1, 3, 5)

    @pl.when(second_entry)
    def _():
        for r in range(n_tp):
            cast_source(OUT, r)

    def project(p):
        made = jnp.dot(normed[...], w_all[p], preferred_element_type=jnp.float32).astype(jnp.bfloat16)
        kv_all[p, pl.ds(rows, 2 * rows), :] = made[:, : 2 * lanes]
        q_buf[p] = (made[:, 2 * lanes :].astype(jnp.float32) * HEAD_DIM ** (-0.5)).astype(jnp.bfloat16)
        pl.when(has_next)(lambda: halo(p).start())

    project(0)
    spread(W1, 6, 7)
    project(1)

    low = lax.broadcasted_iota(jnp.int32, (q_rows, lanes), 1) < HEAD_DIM
    eye = lax.broadcasted_iota(jnp.int32, (q_rows, q_rows), 0) == lax.broadcasted_iota(jnp.int32, (q_rows, q_rows), 1)

    def make_mask(j):
        q_docs = docs_all[pl.ds(0, 1), pl.ds(rows + j * q_rows, q_rows)].astype(jnp.float32)
        k_docs = docs_all[pl.ds(0, 1), pl.ds(j * q_rows, span)].astype(jnp.float32)
        column = jnp.sum(jnp.where(eye, jnp.broadcast_to(q_docs, (q_rows, q_rows)), 0.0), axis=1, keepdims=True)
        mask[j] = jnp.where(column == k_docs, 0.0, NEG)

    def attend_rows(p, j):
        keys = pl.ds(j * q_rows, span)
        q_pair = q_buf[p, pl.ds(j * q_rows, q_rows), :]
        k_pair = kv_all[p, keys, pl.ds(0, lanes)]
        v_pair = kv_all[p, keys, pl.ds(lanes, lanes)]
        both = []
        for half in range(2):
            on = low if half == 0 else jnp.logical_not(low)
            q_one = jnp.where(on, q_pair, jnp.zeros_like(q_pair))
            score = lax.dot_general(q_one, k_pair, (((1,), (1,)), ((), ())), preferred_element_type=jnp.float32)
            score = score + bias[2 * p + half] + mask[j]
            raised = jnp.exp(score - jnp.max(score, axis=-1, keepdims=True))
            total = jnp.sum(raised, axis=-1, keepdims=True)
            both.append(jnp.dot(raised.astype(jnp.bfloat16), v_pair, preferred_element_type=jnp.float32) / total)
        return jnp.where(low, both[0], both[1]).astype(jnp.bfloat16)

    per = blocks // 2

    def attend_half(p, which):
        for j in range(per):
            found = attend_rows(p, which * per + j)
            part = pl.ds(j * q_rows, q_rows)
            att_own[p, which, part, :] = found

            @pl.when(first_entry & (x == which))
            def _():
                att_all[t, part, at_multiple(x * half_cols + p * lanes, lanes, lanes)] = found

        pl.when(x == which)(lambda: send_direct(A0 + p))
        pl.when(x != which)(lambda: send_cross(A0 + p))

    for j in range(per, blocks):
        make_mask(j)
    attend_half(0, 1)

    @pl.when(has_prev)
    def _():
        for i in (pairs, 0):
            halo(i).wait_recv()

    for j in range(per):
        make_mask(j)
    cast_forward(OUT, 0)
    attend_half(0, 0)
    cast_forward(OUT, 1)
    send_relay(A0)
    attend_half(1, 1)
    cast_forward(OUT, 2)
    pl.when(has_prev)(lambda: halo(1).wait_recv())
    attend_half(1, 0)
    cast_forward(OUT, 3)
    send_relay(A1)
    spread(A0, 0, 7)
    spread(A1, 0, 7)
    for r in range(n_tp):
        across_in(OUT, r).wait_recv()
    resid_copy.wait()
    half_chunk = chunk // 2
    for i in range(2):
        made = jnp.zeros((rows, half_chunk), jnp.float32)
        for r in range(n_tp):
            made = made + jnp.dot(att_all[r], wo_all[2 * r + i], preferred_element_type=jnp.float32)
        part = pl.ds(i * half_chunk, half_chunk)
        done[home_y, :, part] = (resid[:, part].astype(jnp.float32) + made).astype(jnp.bfloat16)

    def store(which):
        return pltpu.make_async_copy(
            done.at[which], out_ref.at[:, at_multiple(which * chunk, chunk, chunk)], store_sem.at[which]
        )

    def tp_move(i, which, target):
        return remote(done.at[which], done.at[which], tp_send.at[i], tp_recv.at[i], tp=target)

    out_to_y, out_to_core, pass_on = tp_move(0, home_y, t_y), tp_move(1, home_y, t_core), tp_move(2, home, t_core)
    out_to_y.start()
    out_to_core.start()
    store(home_y).start()
    out_to_y.wait_recv()
    pass_on.start()
    store(home).start()
    out_to_core.wait_recv()
    store(plane_of(t_far)).start()
    pass_on.wait_recv()
    store(plane_of(t_core)).start()
    for which in range(n_tp):
        store(which).wait()

    for ch in range(4):
        drain(ch)
    cast_drain(TOK, pieces + 1)
    cast_drain(OUT, n_tp)

    @pl.when(first_entry)
    def _():
        for i in range(3):
            line_copy(i).wait_send()

    @pl.when(has_next)
    def _():
        for i in range(pairs + 1):
            halo(i).wait_send()
    for one in (out_to_y, out_to_core, pass_on):
        one.wait_send()


def body_one(n_sp, n_tp, tokens, documents, norm_gain, w_query, w_key, w_value, w_out, rel_bias):
    rows, width = tokens.shape
    depth, cols = w_query.shape[1:]
    heads = cols // HEAD_DIM
    out_cols = w_out.shape[2]
    chunk = width // n_tp
    lanes = 2 * HEAD_DIM
    pairs = cols // 2 // lanes
    reach = LEFT * SEG
    table = rel_bias[0]
    furthest = table[:, 2 * REL_CLIP:]
    ahead, behind = reach - REL_CLIP, reach - REL_CLIP - 1
    line = jnp.concatenate(
        [
            jnp.broadcast_to(furthest, (heads, ahead)),
            table[:, ::-1],
            jnp.broadcast_to(furthest, (heads, behind)),
        ],
        axis=1,
    )
    doc_row = jnp.broadcast_to(documents[None, :], (8, rows))
    bf, f32 = jnp.bfloat16, jnp.float32
    vmem = pl.BlockSpec(memory_space=pltpu.VMEM)
    hbm = pl.BlockSpec(memory_space=pl.ANY)
    dma = pltpu.SemaphoreType.DMA
    q_rows, span = 2 * SEG, (LEFT + 2) * SEG
    return pl.pallas_call(
        functools.partial(layer_kernel, n_sp, n_tp),
        out_shape=jax.ShapeDtypeStruct((rows, width), bf),
        in_specs=[vmem] * 3 + [hbm] * 5,
        out_specs=hbm,
        scratch_shapes=[
            pltpu.VMEM((2, pairs, depth, 3 * lanes), bf),
            pltpu.VMEM((pairs, depth, 3 * lanes), bf),
            pltpu.VMEM((pairs, n_sp * depth, 3 * lanes), bf),
            pltpu.VMEM((n_sp, cols, out_cols), bf),
            pltpu.VMEM((2, rows, width), bf),
            pltpu.VMEM((rows, chunk), bf),
            pltpu.VMEM((2 * rows, width), bf),
            pltpu.VMEM(line.shape, f32),
            pltpu.VMEM((heads // 2, q_rows, span), f32),
            pltpu.VMEM((pairs, 2 * rows, lanes), bf),
            pltpu.VMEM((pairs, 3 * rows, 2 * lanes), bf),
            pltpu.VMEM((8, 3 * rows), jnp.int32),
            pltpu.VMEM((2 * rows // q_rows, q_rows, span), f32),
            pltpu.VMEM((pairs, 2, rows, lanes), bf),
            pltpu.VMEM((pairs, rows, lanes), bf),
            pltpu.VMEM((n_tp, rows, cols), bf),
            pltpu.VMEM((n_tp, rows, chunk), bf),
            dma((2, pairs, 3)),
            dma((pairs, 3)),
            dma((n_tp,)),
            dma((n_tp,)),
            dma(()),
            dma((3,)),
            dma(()),
            dma((4, 3)),
            dma((4,)),
            dma((4, 2, n_sp)),
            dma((4, n_sp)),
            dma((2, 3, n_tp + 1)),
            dma((2, 2, n_tp + 1)),
            dma((pairs + 1,)),
            dma((pairs + 1,)),
            dma((3,)),
            dma((3,)),
            dma((n_tp,)),
        ],
        compiler_params=pltpu.CompilerParams(
            collective_id=0, has_side_effects=True, vmem_limit_bytes=60 * 1024 * 1024
        ),
    )(doc_row, norm_gain, line, tokens, w_key[0], w_value[0], w_query[0], w_out[0])


def fits_one(mesh):
    return mesh.shape["tp"] == 4 and mesh.shape["sp"] == 2 * mesh.shape["tp"]


def solution(mesh):
    n_sp, n_tp = mesh.shape["sp"], mesh.shape["tp"]
    run = functools.partial(body_one, n_sp, n_tp) if fits_one(mesh) else body
    in_specs = (
        P("sp", None),
        P("sp"),
        P(),
        P(None, "sp", "tp"),
        P(None, "sp", "tp"),
        P(None, "sp", "tp"),
        P(None, None, "sp"),
        P(None, "tp", None),
    )
    out_specs = P("sp", None)
    return jax.shard_map(run, mesh=mesh, in_specs=in_specs, out_specs=out_specs, check_vma=False)
```

time: 109 us -> 127 us (1.17)
  Pallas kernels: 103 us -> 121 us
    pallas_call x1, Pallas kernels: 103 us -> 121 us  [body_one(): pl.pallas_call(functools.partial(layer_kernel, n_sp, n_tp), out_shape=jax...]
where the time goes in v1:
time: 127 us
  Pallas kernels  121 us (95%)
  local copies, waits for them, and re-layouts  4.82 us (4%)
    pallas_call x1, Pallas kernels, body_one(): pl.pallas_call(functools.partial(layer_kernel, n_sp, n_tp), out_shape=jax...  121 us
    unnamed x7, local copies, waits for them, and re-layouts  3.21 us

profile of v1, /device:TPU:0, one launch (start us, length us, event | category | flops | bytes accessed | tf_op | source)
XLA Modules:
  0.0 126.7 jit_solution(11129093421317495096)
XLA Ops:
  0.0 0.0 copy-start
  0.0 0.9 slice_reduce_fusion
  0.9 0.1 broadcast_in_dim.21
  0.9 0.0 copy-start.1
  0.9 0.1 broadcast_in_dim.20
  1.0 0.6 copy-done.1
  1.6 0.6 broadcast_in_dim.8.doc_row
  2.2 0.0 copy-done
  2.2 0.2 reverse
  2.4 0.1 slice.6
  2.5 0.7 pad_maximum_fusion.line_ref
  3.2 121.2 %shard_map.82 = bf16[256,2048]{1,0:T(8,128)(2,1)} custom-call(s32[8,256]{1,0:T(8,128)} %broadcast_in_dim.8.doc_row, f32[1,2048]{1,0:T(1,128)} %gain_ref.1, f32[8,512]{1,0:T(8,128)} %pad_maximum_fusion.line_ref, bf16[256,2048]{1,0:T(8,128)(2,1)} %x_in.1, bf16[256,512]{1,0:T(8,128)(2,1)} %bitcast.7, bf16[256,512]{1,0:T(8,128)(2,1)} %bitcast.8, ...), custom_call_target="tpu_custom_call" | custom-call | tf_op jit(solution)/shard_map/pallas_call | solution.py:615
  124.4 2.3 %copy.10 = bf16[256,2048]{1,0:T(8,128)(2,1)} copy(bf16[256,2048]{1,0:T(8,128)(2,1)} %shard_map.82) | data formatting | bytes 2097152
Async XLA Ops:
  0.0 2.2 %copy-start = (f32[1,8,257]{2,1,0:T(8,128)S(1)}, f32[1,8,257]{2,1,0:T(8,128)}, u32[]{:S(2)}) copy-start(f32[1,8,257]{2,1,0:T(8,128)} %param.15) | copy-start | bytes 24676
  0.9 0.7 copy-start.1

commit v2 on v1

--- a/solution.py
+++ b/solution.py
@@ -133,10 +133,10 @@
 
 
 def layer_kernel(
-    n_sp, n_tp, doc_row, gain_ref, line_ref, x_in, wk_in, wv_in, wq_in, wo_in, out_ref,
-    w_own, w_relay, w_all, wo_all, tok, resid, normed, line_all, bias, q_buf, kv_all, docs_all, mask,
+    n_sp, n_tp, doc_in, gain_in, table_in, x_in, wk_in, wv_in, wq_in, wo_in, out_ref,
+    w_own, w_relay, w_all, wo_all, tok, aid, wo_aid, resid, normed, gain, table, bias, q_buf, kv_all, docs_all, mask,
     att_own, att_relay, att_all, done,
-    own_sem, loc_sem, out_sem, tok_sem, res_sem, line_send, line_recv, hop_send, relay_recv, rep_send, rep_recv,
+    own_sem, loc_sem, out_sem, tok_sem, aid_sem, aid_send, wo_aid_sem, wo_aid_send, res_sem, small_sem, line_send, line_recv, hop_send, relay_recv, rep_send, rep_recv,
     cast_send, cast_recv, halo_send, halo_recv, tp_send, tp_recv, store_sem,
 ):
     rows, width = tok.shape[1:]
@@ -193,12 +193,19 @@
     def out_copy(r):
         return pltpu.make_async_copy(wo_in.at[pl.ds(r * cols, cols), :], wo_all.at[2 * r + x], out_sem.at[r])
 
+    doc_copy = pltpu.make_async_copy(doc_in, docs_all.at[:, at_multiple((1 + x) * rows, rows, rows)], small_sem.at[0])
+    gain_copy = pltpu.make_async_copy(gain_in, gain, small_sem.at[1])
+    table_copy = pltpu.make_async_copy(table_in, table, small_sem.at[2])
     resid_copy = pltpu.make_async_copy(x_in.at[:, at_multiple(home_y * chunk, chunk, chunk)], resid, res_sem)
 
+    gain_copy.start()
+
     @pl.when(first_entry)
     def _():
+        doc_copy.start()
         for r in range(pieces):
             tok_copy(r).start()
+        table_copy.start()
 
     for p in range(pairs):
         for i in (1, 0):
@@ -211,8 +218,24 @@
             for kind in range(3):
                 local_copy(p, kind).start()
 
+    outer = (z == 0) | (z == nz - 1)
+    inner = jnp.logical_not(outer)
+    lower = z < nz // 2
+    aid_copy = pltpu.make_async_copy(x_in.at[pl.ds(rows // 2, rows // 2), :], aid, aid_sem)
+
+    def wo_aid_copy(r):
+        i = r - n_tp // 2
+        return pltpu.make_async_copy(wo_in.at[pl.ds(r * cols, cols), :], wo_aid.at[i], wo_aid_sem.at[i])
+
+    @pl.when(first_entry & inner)
+    def _():
+        for r in range(n_tp // 2, n_tp):
+            wo_aid_copy(r).start()
+
     @pl.when(second_entry)
     def _():
+        pl.when(inner)(lambda: aid_copy.start())
+
         for r in range(n_tp):
             out_copy(r).start()
 
@@ -342,15 +365,42 @@
 
     centers = (home, home_y)
 
+    def aided(kind, r):
+        return pieces // 2 <= r < pieces
+
+    def goes(kind, way, r):
+        ok = (z >= centers[kind]) & has_up if way == UP else (z <= centers[kind]) & has_down
+        if aided(kind, r):
+            near = jnp.logical_not(lower) if way == UP else lower
+            ok = ok & jnp.logical_not((z == centers[kind]) & inner & near)
+        return ok
+
+    def aid_send_on(r):
+        part = pl.ds((r - pieces // 2) * piece, piece)
+        return remote(
+            aid.at[part, :], cast_ref(TOK, x, r), aid_send.at[r - pieces // 2], cast_recv.at[TOK, x, r],
+            sp=s + 2 - 4 * (1 - z // (nz // 2)), tp=t_y,
+        )
+
+    def wo_aid_send_on(r):
+        i = r - n_tp // 2
+        return remote(
+            wo_aid.at[i], cast_ref(OUT, x, r), wo_aid_send.at[i], cast_recv.at[OUT, x, r],
+            sp=s + 2 - 4 * (1 - z // (nz // 2)), tp=t_y,
+        )
+
+    def cast_along(kind, r, src=None):
+        for way in (UP, DOWN):
+            pl.when(goes(kind, way, r))(lambda: move(kind, way, r, src).start())
+
     def cast_send_on(kind, r, src=None):
-        pl.when((z >= centers[kind]) & has_up)(lambda: move(kind, UP, r, src).start())
-        pl.when((z <= centers[kind]) & has_down)(lambda: move(kind, DOWN, r, src).start())
+        cast_along(kind, r, src)
         move(kind, ACROSS, r, src).start()
 
     def cast_source(kind, r):
         if r == pieces and kind == TOK:
-            docs_all[:, at_multiple((1 + x) * rows, rows, rows)] = doc_row[...]
-            cast_send_on(kind, r, doc_row)
+            doc_copy.wait()
+            cast_send_on(kind, r)
             return
         (tok_copy, out_copy)[kind](r).wait()
         cast_send_on(kind, r)
@@ -363,14 +413,14 @@
 
     def cast_drain(kind, count):
         for r in range(count):
-            pl.when((z >= centers[kind]) & has_up)(lambda: move(kind, UP, r).wait_send())
-            pl.when((z <= centers[kind]) & has_down)(lambda: move(kind, DOWN, r).wait_send())
+            for way in (UP, DOWN):
+                pl.when(goes(kind, way, r))(lambda: move(kind, way, r).wait_send())
             move(kind, ACROSS, r).wait_send()
 
     line_targets = (t_core, t_y, t_far)
 
     def line_copy(i):
-        return remote(line_ref, line_all, line_send.at[i], line_recv, tp=line_targets[i])
+        return remote(table, table, line_send.at[i], line_recv, tp=line_targets[i])
 
     has_next, has_prev = home < nz - 1, home > 0
 
@@ -390,12 +440,10 @@
         pl.semaphore_signal(barrier, inc=1, device_id={"tp": peer}, device_id_type=MESH)
     for peer in (t, t_y):
         pl.semaphore_signal(barrier, inc=1, device_id={"sp": mate, "tp": peer}, device_id_type=MESH)
-    pl.semaphore_wait(barrier, nz + 4)
-
-    @pl.when(first_entry)
-    def _():
-        cast_source(TOK, pieces)
-        cast_source(TOK, 0)
+    pl.semaphore_signal(
+        barrier, inc=1, device_id={"sp": s + 2 - 4 * (z % 2), "tp": t_y}, device_id_type=MESH
+    )
+    pl.semaphore_wait(barrier, nz + 5)
 
     for p in range(pairs):
         for i in (1, 0):
@@ -405,49 +453,152 @@
 
     @pl.when(first_entry)
     def _():
-        for r in range(1, pieces):
+        for r in (pieces,) + tuple(range(pieces // 2)):
             cast_source(TOK, r)
+        table_copy.wait()
         for i in range(3):
             line_copy(i).start()
 
+    def out_along(r):
+        out_copy(r).wait()
+        cast_along(OUT, r)
+
+    def out_near(r):
+        pl.when(goes(OUT, UP, r) & jnp.logical_not(lower))(lambda: move(OUT, UP, r).start())
+        pl.when(goes(OUT, DOWN, r) & lower)(lambda: move(OUT, DOWN, r).start())
+
+    def out_far(r):
+        pl.when(goes(OUT, UP, r) & lower)(lambda: move(OUT, UP, r).start())
+        pl.when(goes(OUT, DOWN, r) & jnp.logical_not(lower))(lambda: move(OUT, DOWN, r).start())
+
+    def out_across(r):
+        move(OUT, ACROSS, r).start()
+
+    def out_pass(r):
+        @pl.when(z != home_y)
+        def _():
+            move(OUT, UP, r).wait_recv()
+            cast_along(OUT, r)
+
+    @pl.when(second_entry)
+    def _():
+        @pl.when(inner)
+        def _():
+            aid_copy.wait()
+            for r in range(pieces // 2, pieces):
+                aid_send_on(r).start()
+
+        @pl.when(outer)
+        def _():
+            for r in range(n_tp):
+                out_along(r)
+            out_across(0)
+
     @pl.when(has_prev == False)
     def _():
-        docs_all[:, pl.ds(0, rows)] = jnp.full((8, rows), -1, jnp.int32)
+        docs_all[:, pl.ds(0, rows)] = jnp.full((1, rows), -1, jnp.int32)
         for p in range(pairs):
             kv_all[p, pl.ds(0, rows), :] = jnp.zeros((rows, 2 * lanes), jnp.bfloat16)
 
-    send_relay(W0)
-    cast_forward(TOK, pieces)
-    cast_forward(TOK, 0)
-    send_relay(W1)
-    spread(W0, 0, 0)
-    cast_forward(TOK, 1)
-    spread(W0, 1, 2)
-    cast_forward(TOK, 2)
-    spread(W0, 3, 4)
-    cast_forward(TOK, 3)
-    spread(W0, 5, 7)
+    def around(d):
+        return (0,) if d == 0 else (-d, d)
+
+    def pass_mine(ch, d):
+        for off in around(d):
+            mine(ch, off)
+
+    def pass_theirs(ch, d):
+        for off in around(d):
+            theirs(ch, off)
+
+    @pl.when(first_entry)
+    def _():
+        pass_mine(W0, 0)
+        pass_mine(W1, 0)
+        send_relay(W0)
+        send_relay(W1)
+        for r in range(pieces // 2, pieces):
+            cast_source(TOK, r)
+        for ch in (W0, W1):
+            for d in range(1, nz):
+                pass_mine(ch, d)
+
+        @pl.when(inner)
+        def _():
+            for r in range(n_tp):
+                out_pass(r)
+
+        for ch in (W0, W1):
+            for d in range(nz):
+                pass_theirs(ch, d)
+
+    @pl.when(second_entry)
+    def _():
+        pass_mine(W0, 0)
+        cast_forward(TOK, pieces)
+        cast_forward(TOK, 0)
+        pass_mine(W1, 0)
+        cast_forward(TOK, 1)
+        pass_mine(W0, 1)
+        pass_mine(W1, 1)
+        cast_forward(TOK, 2)
+        pass_mine(W0, 2)
+        pass_mine(W1, 2)
+        cast_forward(TOK, 3)
+        pass_mine(W0, 3)
+        pass_mine(W1, 3)
+
+        @pl.when(inner)
+        def _():
+            for r in range(n_tp):
+                out_copy(r).wait()
+                out_far(r)
+            out_across(0)
+
+        for ch in (W0, W1):
+            for d in range(nz):
+                pass_theirs(ch, d)
+
+    @pl.when(jnp.logical_not(entry))
+    def _():
+        send_relay(W0)
+        send_relay(W1)
+        for r in (pieces,) + tuple(range(pieces)):
+            cast_forward(TOK, r)
+        pl.when(inner)(lambda: out_pass(0))
+        for ch in (W0, W1):
+            for d in range(nz):
+                pass_theirs(ch, d)
+
+
+    gain_copy.wait()
 
     def normalize(which):
         wide = tok[which].astype(jnp.float32)
         normed[at_multiple(which * rows, rows, rows), :] = (
-            wide * lax.rsqrt(jnp.mean(wide * wide, axis=-1, keepdims=True) + EPS) * gain_ref[...]
+            wide * lax.rsqrt(jnp.mean(wide * wide, axis=-1, keepdims=True) + EPS) * gain[...]
         ).astype(jnp.bfloat16)
 
     normalize(x)
-    spread(W1, 0, 2)
 
     q_rows, span = 2 * SEG, (LEFT + 2) * SEG
     heads = half_cols // HEAD_DIM
     blocks = 2 * rows // q_rows
 
-    pl.when(first_entry)(lambda: line_all.__setitem__(Ellipsis, line_ref[...]))
     pl.when(jnp.logical_not(first_entry))(lambda: line_copy(0).wait_recv())
     q_seg = lax.broadcasted_iota(jnp.int32, (q_rows, span), 0) // SEG
     k_seg = lax.broadcasted_iota(jnp.int32, (q_rows, span), 1) // SEG
     near = (k_seg >= q_seg) & (k_seg <= q_seg + LEFT)
+    length = table.shape[1]
+    line_len = (LEFT + 4) * SEG
+    entry_of = lax.broadcasted_iota(jnp.int32, (length, line_len), 0)
+    back = LEFT * SEG - lax.broadcasted_iota(jnp.int32, (length, line_len), 1)
+    back = jnp.where(back < -REL_CLIP, REL_CLIP, jnp.minimum(back, REL_CLIP))
+    pick = (entry_of == back + REL_CLIP).astype(jnp.float32)
+    lines = jnp.dot(table[...], pick, precision=lax.Precision.HIGHEST, preferred_element_type=jnp.float32)
+    lines = jnp.where(x == 0, lines[:heads], lines[heads:])
     for h in range(heads):
-        line = jnp.broadcast_to(line_all[pl.ds(x * heads + h, 1), :], (q_rows, line_ref.shape[1]))
+        line = jnp.broadcast_to(lines[h : h + 1, :], (q_rows, line_len))
         skew = pltpu.roll(line, 0, 1, stride=1, stride_axis=0)
         bias[h] = jnp.where(near, skew[:, :span], NEG)
 
@@ -455,12 +606,6 @@
         across_in(TOK, r).wait_recv()
     normalize(1 - x)
     pl.when(has_next)(lambda: halo(pairs).start())
-    spread(W1, 3, 5)
-
-    @pl.when(second_entry)
-    def _():
-        for r in range(n_tp):
-            cast_source(OUT, r)
 
     def project(p):
         made = jnp.dot(normed[...], w_all[p], preferred_element_type=jnp.float32).astype(jnp.bfloat16)
@@ -468,9 +613,27 @@
         q_buf[p] = (made[:, 2 * lanes :].astype(jnp.float32) * HEAD_DIM ** (-0.5)).astype(jnp.bfloat16)
         pl.when(has_next)(lambda: halo(p).start())
 
+    middle = jnp.logical_not(entry) & inner
+    late = jnp.logical_not(second_entry) & outer
     project(0)
-    spread(W1, 6, 7)
+    pl.when(middle)(lambda: out_pass(1))
     project(1)
+
+    @pl.when(middle)
+    def _():
+        out_pass(2)
+        out_pass(3)
+
+    @pl.when(second_entry & inner)
+    def _():
+        for r in range(n_tp):
+            out_near(r)
+
+    @pl.when(first_entry & inner)
+    def _():
+        for r in range(n_tp // 2, n_tp):
+            wo_aid_copy(r).wait()
+            wo_aid_send_on(r).start()
 
     low = lax.broadcasted_iota(jnp.int32, (q_rows, lanes), 1) < HEAD_DIM
     eye = lax.broadcasted_iota(jnp.int32, (q_rows, q_rows), 0) == lax.broadcasted_iota(jnp.int32, (q_rows, q_rows), 1)
@@ -523,56 +686,85 @@
 
     for j in range(per):
         make_mask(j)
-    cast_forward(OUT, 0)
     attend_half(0, 0)
-    cast_forward(OUT, 1)
+    pl.when(late)(lambda: out_pass(0))
+    pl.when(jnp.logical_not(second_entry))(lambda: out_across(0))
+    attend_half(1, 1)
     send_relay(A0)
-    attend_half(1, 1)
-    cast_forward(OUT, 2)
     pl.when(has_prev)(lambda: halo(1).wait_recv())
     attend_half(1, 0)
-    cast_forward(OUT, 3)
+    pl.when(late)(lambda: out_pass(1))
+    out_across(1)
     send_relay(A1)
-    spread(A0, 0, 7)
-    spread(A1, 0, 7)
-    for r in range(n_tp):
-        across_in(OUT, r).wait_recv()
-    resid_copy.wait()
+    pl.when(late)(lambda: out_pass(2))
+    out_across(2)
+    pl.when(late)(lambda: out_pass(3))
+    out_across(3)
+
+    for ch in (A0, A1):
+        for d in range(nz):
+            pass_mine(ch, d)
+    for ch in (A0, A1):
+        for d in range(nz):
+            pass_theirs(ch, d)
+
     half_chunk = chunk // 2
-    for i in range(2):
+
+    def store(which, i):
+        return pltpu.make_async_copy(
+            done.at[which, i], out_ref.at[:, at_multiple(which * chunk + i * half_chunk, half_chunk, half_chunk)],
+            store_sem.at[which, i],
+        )
+
+    def tp_move(way, i):
+        which, target = ((home_y, t_y), (home_y, t_core), (home, t_core))[way]
+        ref = done.at[which, i]
+        return remote(ref, ref, tp_send.at[way, i], tp_recv.at[way, i], tp=target)
+
+    def out_project(i):
         made = jnp.zeros((rows, half_chunk), jnp.float32)
         for r in range(n_tp):
             made = made + jnp.dot(att_all[r], wo_all[2 * r + i], preferred_element_type=jnp.float32)
-        part = pl.ds(i * half_chunk, half_chunk)
-        done[home_y, :, part] = (resid[:, part].astype(jnp.float32) + made).astype(jnp.bfloat16)
-
-    def store(which):
-        return pltpu.make_async_copy(
-            done.at[which], out_ref.at[:, at_multiple(which * chunk, chunk, chunk)], store_sem.at[which]
-        )
-
-    def tp_move(i, which, target):
-        return remote(done.at[which], done.at[which], tp_send.at[i], tp_recv.at[i], tp=target)
-
-    out_to_y, out_to_core, pass_on = tp_move(0, home_y, t_y), tp_move(1, home_y, t_core), tp_move(2, home, t_core)
-    out_to_y.start()
-    out_to_core.start()
-    store(home_y).start()
-    out_to_y.wait_recv()
-    pass_on.start()
-    store(home).start()
-    out_to_core.wait_recv()
-    store(plane_of(t_far)).start()
-    pass_on.wait_recv()
-    store(plane_of(t_core)).start()
+        part = at_multiple(i * half_chunk, half_chunk, half_chunk)
+        done[home_y, i] = (resid[:, part].astype(jnp.float32) + made).astype(jnp.bfloat16)
+        tp_move(0, i).start()
+        tp_move(1, i).start()
+        store(home_y, i).start()
+
+    resid_copy.wait()
+    out_project(x)
+    for r in range(n_tp):
+        across_in(OUT, r).wait_recv()
+    out_project(1 - x)
+    for i in (x, 1 - x):
+        tp_move(0, i).wait_recv()
+        tp_move(2, i).start()
+        store(home, i).start()
+    for i in (x, 1 - x):
+        tp_move(1, i).wait_recv()
+        store(plane_of(t_far), i).start()
+    for i in (x, 1 - x):
+        tp_move(2, i).wait_recv()
+        store(plane_of(t_core), i).start()
     for which in range(n_tp):
-        store(which).wait()
+        for i in range(2):
+            store(which, i).wait()
 
     for ch in range(4):
         drain(ch)
     cast_drain(TOK, pieces + 1)
     cast_drain(OUT, n_tp)
 
+    @pl.when(second_entry & inner)
+    def _():
+        for r in range(pieces // 2, pieces):
+            aid_send_on(r).wait_send()
+
+    @pl.when(first_entry & inner)
+    def _():
+        for r in range(n_tp // 2, n_tp):
+            wo_aid_send_on(r).wait_send()
+
     @pl.when(first_entry)
     def _():
         for i in range(3):
@@ -582,8 +774,9 @@
     def _():
         for i in range(pairs + 1):
             halo(i).wait_send()
-    for one in (out_to_y, out_to_core, pass_on):
-        one.wait_send()
+    for way in range(3):
+        for i in range(2):
+            tp_move(way, i).wait_send()
 
 
 def body_one(n_sp, n_tp, tokens, documents, norm_gain, w_query, w_key, w_value, w_out, rel_bias):
@@ -594,28 +787,15 @@
     chunk = width // n_tp
     lanes = 2 * HEAD_DIM
     pairs = cols // 2 // lanes
-    reach = LEFT * SEG
     table = rel_bias[0]
-    furthest = table[:, 2 * REL_CLIP:]
-    ahead, behind = reach - REL_CLIP, reach - REL_CLIP - 1
-    line = jnp.concatenate(
-        [
-            jnp.broadcast_to(furthest, (heads, ahead)),
-            table[:, ::-1],
-            jnp.broadcast_to(furthest, (heads, behind)),
-        ],
-        axis=1,
-    )
-    doc_row = jnp.broadcast_to(documents[None, :], (8, rows))
     bf, f32 = jnp.bfloat16, jnp.float32
-    vmem = pl.BlockSpec(memory_space=pltpu.VMEM)
     hbm = pl.BlockSpec(memory_space=pl.ANY)
     dma = pltpu.SemaphoreType.DMA
     q_rows, span = 2 * SEG, (LEFT + 2) * SEG
     return pl.pallas_call(
         functools.partial(layer_kernel, n_sp, n_tp),
         out_shape=jax.ShapeDtypeStruct((rows, width), bf),
-        in_specs=[vmem] * 3 + [hbm] * 5,
+        in_specs=[hbm] * 8,
         out_specs=hbm,
         scratch_shapes=[
             pltpu.VMEM((2, pairs, depth, 3 * lanes), bf),
@@ -623,23 +803,31 @@
             pltpu.VMEM((pairs, n_sp * depth, 3 * lanes), bf),
             pltpu.VMEM((n_sp, cols, out_cols), bf),
             pltpu.VMEM((2, rows, width), bf),
+            pltpu.VMEM((rows // 2, width), bf),
+            pltpu.VMEM((n_tp // 2, cols, out_cols), bf),
             pltpu.VMEM((rows, chunk), bf),
             pltpu.VMEM((2 * rows, width), bf),
-            pltpu.VMEM(line.shape, f32),
+            pltpu.VMEM((1, width), f32),
+            pltpu.VMEM(table.shape, f32),
             pltpu.VMEM((heads // 2, q_rows, span), f32),
             pltpu.VMEM((pairs, 2 * rows, lanes), bf),
             pltpu.VMEM((pairs, 3 * rows, 2 * lanes), bf),
-            pltpu.VMEM((8, 3 * rows), jnp.int32),
+            pltpu.VMEM((1, 3 * rows), jnp.int32),
             pltpu.VMEM((2 * rows // q_rows, q_rows, span), f32),
             pltpu.VMEM((pairs, 2, rows, lanes), bf),
             pltpu.VMEM((pairs, rows, lanes), bf),
             pltpu.VMEM((n_tp, rows, cols), bf),
-            pltpu.VMEM((n_tp, rows, chunk), bf),
+            pltpu.VMEM((n_tp, 2, rows, chunk // 2), bf),
             dma((2, pairs, 3)),
             dma((pairs, 3)),
             dma((n_tp,)),
             dma((n_tp,)),
             dma(()),
+            dma((n_tp // 2,)),
+            dma((n_tp // 2,)),
+            dma((n_tp // 2,)),
+            dma(()),
+            dma((3,)),
             dma((3,)),
             dma(()),
             dma((4, 3)),
@@ -650,14 +838,14 @@
             dma((2, 2, n_tp + 1)),
             dma((pairs + 1,)),
             dma((pairs + 1,)),
-            dma((3,)),
-            dma((3,)),
-            dma((n_tp,)),
+            dma((3, 2)),
+            dma((3, 2)),
+            dma((n_tp, 2)),
         ],
         compiler_params=pltpu.CompilerParams(
             collective_id=0, has_side_effects=True, vmem_limit_bytes=60 * 1024 * 1024
         ),
-    )(doc_row, norm_gain, line, tokens, w_key[0], w_value[0], w_query[0], w_out[0])
+    )(documents[None, :], norm_gain, table, tokens, w_key[0], w_value[0], w_query[0], w_out[0])
 
 
 def fits_one(mesh):

time: 127 us -> 88.8 us (0.70)
  Pallas kernels: 121 us -> 85.2 us
  local copies, waits for them, and re-layouts: 4.82 us -> 2.3 us
    pallas_call x1, Pallas kernels: 121 us -> 85.2 us  [body_one(): pl.pallas_call(functools.partial(layer_kernel, n_sp, n_tp), out_shape=jax...]
    unnamed x7 -> x1, local copies, waits for them, and re-layouts: 3.21 us -> 2.3 us
where the time goes in v2:
time: 88.8 us; the launch traced here: 87.5 us
  Pallas kernels  85.2 us (96%)
  local copies, waits for them, and re-layouts  2.3 us (3%)
    pallas_call x1, Pallas kernels, body_one(): pl.pallas_call(functools.partial(layer_kernel, n_sp, n_tp), out_shape=jax...  85.2 us
    unnamed x1, local copies, waits for them, and re-layouts  2.3 us

profile of v2, /device:TPU:0, one launch (start us, length us, event | category | flops | bytes accessed | tf_op | source)
XLA Modules:
  0.0 87.5 jit_solution(8071086269912152631)
XLA Ops:
  0.0 85.2 %shard_map.82 = bf16[256,2048]{1,0:T(8,128)(2,1)} custom-call(s32[1,256]{1,0:T(1,128)} %bitcast.11, f32[1,2048]{1,0:T(1,128)} %gain_in.1, f32[8,257]{1,0:T(8,128)} %bitcast.10, bf16[256,2048]{1,0:T(8,128)(2,1)} %x_in.1, bf16[256,512]{1,0:T(8,128)(2,1)} %bitcast.7, bf16[256,512]{1,0:T(8,128)(2,1)} %bitcast.8, bf16[256,512]{1,0:T(8,128)(2,1)} %bitcast.9, ...), custom_call_target="tpu_custom_call" | custom-call | tf_op jit(solution)/shard_map/pallas_call | solution.py:795
  85.2 2.3 %copy.10 = bf16[256,2048]{1,0:T(8,128)(2,1)} copy(bf16[256,2048]{1,0:T(8,128)(2,1)} %shard_map.82) | data formatting | bytes 2097152

commit v3 on v2

--- a/solution.py
+++ b/solution.py
@@ -135,18 +135,19 @@
 def layer_kernel(
     n_sp, n_tp, doc_in, gain_in, table_in, x_in, wk_in, wv_in, wq_in, wo_in, out_ref,
     w_own, w_relay, w_all, wo_all, tok, aid, wo_aid, resid, normed, gain, table, bias, q_buf, kv_all, docs_all, mask,
-    att_own, att_relay, att_all, done,
+    att_own, att_relay, att_all,
     own_sem, loc_sem, out_sem, tok_sem, aid_sem, aid_send, wo_aid_sem, wo_aid_send, res_sem, small_sem, line_send, line_recv, hop_send, relay_recv, rep_send, rep_recv,
-    cast_send, cast_recv, halo_send, halo_recv, tp_send, tp_recv, store_sem,
+    cast_send, cast_recv, halo_send, halo_recv, tp_send, tp_recv,
 ):
     rows, width = tok.shape[1:]
     depth, cols = wk_in.shape
     half_cols = cols // 2
     lanes = 2 * HEAD_DIM
     pairs = half_cols // lanes
+    q_rows, span = 2 * SEG, (LEFT + 2) * SEG
     chunk = width // n_tp
     nz = n_sp // 2
-    pieces = n_tp
+    pieces = 2 * n_tp
     piece = rows // pieces
     s = lax.axis_index("sp")
     t = lax.axis_index("tp")
@@ -221,15 +222,16 @@
     outer = (z == 0) | (z == nz - 1)
     inner = jnp.logical_not(outer)
     lower = z < nz // 2
-    aid_copy = pltpu.make_async_copy(x_in.at[pl.ds(rows // 2, rows // 2), :], aid, aid_sem)
+    aid_copy = pltpu.make_async_copy(x_in.at[pl.ds(rows - 4 * piece, 4 * piece), :], aid, aid_sem)
 
     def wo_aid_copy(r):
-        i = r - n_tp // 2
-        return pltpu.make_async_copy(wo_in.at[pl.ds(r * cols, cols), :], wo_aid.at[i], wo_aid_sem.at[i])
-
-    @pl.when(first_entry & inner)
-    def _():
-        for r in range(n_tp // 2, n_tp):
+        return pltpu.make_async_copy(wo_in.at[pl.ds(r * cols, cols), :], wo_aid.at[r - 1], wo_aid_sem.at[r - 1])
+
+    aide = inner & (z == plane_of(t_far))
+
+    @pl.when(aide)
+    def _():
+        for r in range(1, n_tp):
             wo_aid_copy(r).start()
 
     @pl.when(second_entry)
@@ -249,8 +251,9 @@
     def slot(ch, block):
         if ch < A0:
             return w_all.at[ch - W0, at_multiple(block * depth, depth, depth), :]
-        start = (block % 2) * half_cols + (ch - A0) * lanes
-        return att_all.at[part_for(block // 2), :, at_multiple(start, lanes, lanes)]
+        return att_all.at[
+            part_for(block // 2), pl.ds((ch - A0) * q_rows, q_rows), at_multiple((block % 2) * half_cols, half_cols, half_cols)
+        ]
 
     def own_ref(ch, i):
         return w_own.at[i, ch - W0] if ch < A0 else att_own.at[ch - A0, x if i == 0 else 1 - x]
@@ -366,7 +369,7 @@
     centers = (home, home_y)
 
     def aided(kind, r):
-        return pieces // 2 <= r < pieces
+        return pieces - 4 <= r < pieces if kind == TOK else r > 0
 
     def goes(kind, way, r):
         ok = (z >= centers[kind]) & has_up if way == UP else (z <= centers[kind]) & has_down
@@ -375,18 +378,17 @@
             ok = ok & jnp.logical_not((z == centers[kind]) & inner & near)
         return ok
 
-    def aid_send_on(r):
-        part = pl.ds((r - pieces // 2) * piece, piece)
+    def aid_move(i):
+        r = pieces - 4 + i
         return remote(
-            aid.at[part, :], cast_ref(TOK, x, r), aid_send.at[r - pieces // 2], cast_recv.at[TOK, x, r],
+            aid.at[pl.ds(i * piece, piece), :], cast_ref(TOK, x, r), aid_send.at[i], cast_recv.at[TOK, x, r],
             sp=s + 2 - 4 * (1 - z // (nz // 2)), tp=t_y,
         )
 
-    def wo_aid_send_on(r):
-        i = r - n_tp // 2
+    def wo_aid_move(r):
         return remote(
-            wo_aid.at[i], cast_ref(OUT, x, r), wo_aid_send.at[i], cast_recv.at[OUT, x, r],
-            sp=s + 2 - 4 * (1 - z // (nz // 2)), tp=t_y,
+            wo_aid.at[r - 1], cast_ref(OUT, x, r), wo_aid_send.at[r - 1], cast_recv.at[OUT, x, r],
+            sp=s + 2 - 4 * (1 - z // (nz // 2)), tp=t_core,
         )
 
     def cast_along(kind, r, src=None):
@@ -443,7 +445,10 @@
     pl.semaphore_signal(
         barrier, inc=1, device_id={"sp": s + 2 - 4 * (z % 2), "tp": t_y}, device_id_type=MESH
     )
-    pl.semaphore_wait(barrier, nz + 5)
+    pl.semaphore_signal(
+        barrier, inc=1, device_id={"sp": s + 2 - 4 * (z % 2), "tp": t_core}, device_id_type=MESH
+    )
+    pl.semaphore_wait(barrier, nz + 6)
 
     for p in range(pairs):
         for i in (1, 0):
@@ -453,7 +458,7 @@
 
     @pl.when(first_entry)
     def _():
-        for r in (pieces,) + tuple(range(pieces // 2)):
+        for r in (pieces,) + tuple(range(pieces)):
             cast_source(TOK, r)
         table_copy.wait()
         for i in range(3):
@@ -485,14 +490,13 @@
         @pl.when(inner)
         def _():
             aid_copy.wait()
-            for r in range(pieces // 2, pieces):
-                aid_send_on(r).start()
+            for i in range(4):
+                aid_move(i).start()
 
         @pl.when(outer)
         def _():
             for r in range(n_tp):
                 out_along(r)
-            out_across(0)
 
     @pl.when(has_prev == False)
     def _():
@@ -517,8 +521,6 @@
         pass_mine(W1, 0)
         send_relay(W0)
         send_relay(W1)
-        for r in range(pieces // 2, pieces):
-            cast_source(TOK, r)
         for ch in (W0, W1):
             for d in range(1, nz):
                 pass_mine(ch, d)
@@ -527,6 +529,13 @@
         def _():
             for r in range(n_tp):
                 out_pass(r)
+                if r < 2:
+                    out_across(r)
+
+        @pl.when(outer)
+        def _():
+            out_pass(0)
+            out_across(0)
 
         for ch in (W0, W1):
             for d in range(nz):
@@ -536,24 +545,37 @@
     def _():
         pass_mine(W0, 0)
         cast_forward(TOK, pieces)
-        cast_forward(TOK, 0)
+        for r in range(0, 2):
+            cast_forward(TOK, r)
+
+        @pl.when(inner)
+        def _():
+            out_copy(0).wait()
+            out_near(0)
+
+        out_across(0)
         pass_mine(W1, 0)
-        cast_forward(TOK, 1)
+        for r in range(2, 4):
+            cast_forward(TOK, r)
+        pl.when(inner)(lambda: out_copy(1).wait())
+        out_across(1)
         pass_mine(W0, 1)
         pass_mine(W1, 1)
-        cast_forward(TOK, 2)
+        for r in range(4, 6):
+            cast_forward(TOK, r)
         pass_mine(W0, 2)
         pass_mine(W1, 2)
-        cast_forward(TOK, 3)
+        for r in range(6, 8):
+            cast_forward(TOK, r)
         pass_mine(W0, 3)
         pass_mine(W1, 3)
 
         @pl.when(inner)
         def _():
             for r in range(n_tp):
-                out_copy(r).wait()
+                if r >= 2:
+                    out_copy(r).wait()
                 out_far(r)
-            out_across(0)
 
         for ch in (W0, W1):
             for d in range(nz):
@@ -565,6 +587,13 @@
         send_relay(W1)
         for r in (pieces,) + tuple(range(pieces)):
             cast_forward(TOK, r)
+
+        @pl.when(aide)
+        def _():
+            for r in range(1, n_tp):
+                wo_aid_copy(r).wait()
+                wo_aid_move(r).start()
+
         pl.when(inner)(lambda: out_pass(0))
         for ch in (W0, W1):
             for d in range(nz):
@@ -581,7 +610,6 @@
 
     normalize(x)
 
-    q_rows, span = 2 * SEG, (LEFT + 2) * SEG
     heads = half_cols // HEAD_DIM
     blocks = 2 * rows // q_rows
 
@@ -602,38 +630,29 @@
         skew = pltpu.roll(line, 0, 1, stride=1, stride_axis=0)
         bias[h] = jnp.where(near, skew[:, :span], NEG)
 
+    def project(which):
+        own = at_multiple(which * rows, rows, rows)
+        for p in range(pairs):
+            made = jnp.dot(normed[own, :], w_all[p], preferred_element_type=jnp.float32).astype(jnp.bfloat16)
+            kv_all[p, at_multiple((1 + which) * rows, rows, rows), :] = made[:, : 2 * lanes]
+            q_buf[p, own, :] = (made[:, 2 * lanes :].astype(jnp.float32) * HEAD_DIM ** (-0.5)).astype(jnp.bfloat16)
+
+    def send_halo():
+        for p in range(pairs):
+            halo(p).start()
+
+    project(x)
+    pl.when(has_next & (x == 1))(send_halo)
+    middle = jnp.logical_not(entry) & inner
+
+    pl.when(middle)(lambda: out_pass(1))
     for r in range(pieces + 1):
         across_in(TOK, r).wait_recv()
+    pl.when(has_next)(lambda: halo(pairs).start())
     normalize(1 - x)
-    pl.when(has_next)(lambda: halo(pairs).start())
-
-    def project(p):
-        made = jnp.dot(normed[...], w_all[p], preferred_element_type=jnp.float32).astype(jnp.bfloat16)
-        kv_all[p, pl.ds(rows, 2 * rows), :] = made[:, : 2 * lanes]
-        q_buf[p] = (made[:, 2 * lanes :].astype(jnp.float32) * HEAD_DIM ** (-0.5)).astype(jnp.bfloat16)
-        pl.when(has_next)(lambda: halo(p).start())
-
-    middle = jnp.logical_not(entry) & inner
     late = jnp.logical_not(second_entry) & outer
-    project(0)
-    pl.when(middle)(lambda: out_pass(1))
-    project(1)
-
-    @pl.when(middle)
-    def _():
-        out_pass(2)
-        out_pass(3)
-
-    @pl.when(second_entry & inner)
-    def _():
-        for r in range(n_tp):
-            out_near(r)
-
-    @pl.when(first_entry & inner)
-    def _():
-        for r in range(n_tp // 2, n_tp):
-            wo_aid_copy(r).wait()
-            wo_aid_send_on(r).start()
+    project(1 - x)
+    pl.when(has_next & (x == 0))(send_halo)
 
     low = lax.broadcasted_iota(jnp.int32, (q_rows, lanes), 1) < HEAD_DIM
     eye = lax.broadcasted_iota(jnp.int32, (q_rows, q_rows), 0) == lax.broadcasted_iota(jnp.int32, (q_rows, q_rows), 1)
@@ -644,111 +663,117 @@
         column = jnp.sum(jnp.where(eye, jnp.broadcast_to(q_docs, (q_rows, q_rows)), 0.0), axis=1, keepdims=True)
         mask[j] = jnp.where(column == k_docs, 0.0, NEG)
 
-    def attend_rows(p, j):
-        keys = pl.ds(j * q_rows, span)
-        q_pair = q_buf[p, pl.ds(j * q_rows, q_rows), :]
-        k_pair = kv_all[p, keys, pl.ds(0, lanes)]
-        v_pair = kv_all[p, keys, pl.ds(lanes, lanes)]
-        both = []
-        for half in range(2):
-            on = low if half == 0 else jnp.logical_not(low)
-            q_one = jnp.where(on, q_pair, jnp.zeros_like(q_pair))
-            score = lax.dot_general(q_one, k_pair, (((1,), (1,)), ((), ())), preferred_element_type=jnp.float32)
-            score = score + bias[2 * p + half] + mask[j]
-            raised = jnp.exp(score - jnp.max(score, axis=-1, keepdims=True))
-            total = jnp.sum(raised, axis=-1, keepdims=True)
-            both.append(jnp.dot(raised.astype(jnp.bfloat16), v_pair, preferred_element_type=jnp.float32) / total)
-        return jnp.where(low, both[0], both[1]).astype(jnp.bfloat16)
+    def attend_rows(g):
+        keys, queries = pl.ds(g * q_rows, span), pl.ds(g * q_rows, q_rows)
+        found = []
+        for p in range(pairs):
+            q_pair = q_buf[p, queries, :]
+            k_pair = kv_all[p, keys, pl.ds(0, lanes)]
+            v_pair = kv_all[p, keys, pl.ds(lanes, lanes)]
+            both = []
+            for half in range(2):
+                on = low if half == 0 else jnp.logical_not(low)
+                q_one = jnp.where(on, q_pair, jnp.zeros_like(q_pair))
+                score = lax.dot_general(q_one, k_pair, (((1,), (1,)), ((), ())), preferred_element_type=jnp.float32)
+                score = score + bias[2 * p + half] + mask[g]
+                raised = jnp.exp(score - jnp.max(score, axis=-1, keepdims=True))
+                total = jnp.sum(raised, axis=-1, keepdims=True)
+                both.append(jnp.dot(raised.astype(jnp.bfloat16), v_pair, preferred_element_type=jnp.float32) / total)
+            found.append(jnp.where(low, both[0], both[1]).astype(jnp.bfloat16))
+        return jnp.concatenate(found, axis=1)
 
     per = blocks // 2
 
-    def attend_half(p, which):
-        for j in range(per):
-            found = attend_rows(p, which * per + j)
-            part = pl.ds(j * q_rows, q_rows)
-            att_own[p, which, part, :] = found
-
-            @pl.when(first_entry & (x == which))
-            def _():
-                att_all[t, part, at_multiple(x * half_cols + p * lanes, lanes, lanes)] = found
-
-        pl.when(x == which)(lambda: send_direct(A0 + p))
-        pl.when(x != which)(lambda: send_cross(A0 + p))
-
-    for j in range(per, blocks):
-        make_mask(j)
-    attend_half(0, 1)
+    def attend_step(j, which):
+        found = attend_rows(which * per + j)
+        att_own[j, which] = found
+
+        @pl.when(first_entry & (x == which))
+        def _():
+            att_all[t, pl.ds(j * q_rows, q_rows), at_multiple(x * half_cols, half_cols, half_cols)] = found
+
+        pl.when(x == which)(lambda: send_direct(A0 + j))
+        pl.when(x != which)(lambda: send_cross(A0 + j))
+
+    for g in range(per, blocks):
+        make_mask(g)
+    attend_step(0, 1)
+    pl.when(middle)(lambda: out_pass(2))
+    attend_step(1, 1)
+    pl.when(middle)(lambda: out_pass(3))
 
     @pl.when(has_prev)
     def _():
-        for i in (pairs, 0):
+        for i in (pairs,) + tuple(range(pairs)):
             halo(i).wait_recv()
 
+    for g in range(per):
+        make_mask(g)
+    attend_step(0, 0)
+    attend_step(1, 0)
+    third = jnp.logical_not(entry)
+    pl.when(third & outer)(lambda: out_pass(0))
+    pl.when(third)(lambda: out_across(0))
+    pl.when(first_entry & outer)(lambda: out_pass(1))
+    pl.when(first_entry & outer)(lambda: out_across(1))
+    send_relay(A0)
+    send_relay(A1)
+    pl.when(third & outer)(lambda: out_pass(1))
+    pl.when(third)(lambda: out_across(1))
+    swift = jnp.logical_not(late)
+
+    @pl.when(swift)
+    def _():
+        out_across(2)
+        out_across(3)
+
+    for d in range(nz):
+        for ch in (A0, A1):
+            pass_mine(ch, d)
+
+    @pl.when(late)
+    def _():
+        for r in (2, 3):
+            out_pass(r)
+            out_across(r)
+
+    half_chunk = chunk // 2
+
+    def result(which, j, i):
+        cut = at_multiple(which * chunk + i * half_chunk, half_chunk, half_chunk)
+        return out_ref.at[pl.ds(j * q_rows, q_rows), cut]
+
+    def tp_move(way, j, i):
+        which, target = ((home_y, t_y), (home_y, t_core), (home, t_core))[way]
+        ref = result(which, j, i)
+        return remote(ref, ref, tp_send.at[way, j, i], tp_recv.at[way, j, i], tp=target)
+
+    def out_project(j, i):
+        part = pl.ds(j * q_rows, q_rows)
+        made = jnp.zeros((q_rows, half_chunk), jnp.float32)
+        for r in range(n_tp):
+            made = made + jnp.dot(att_all[r, part, :], wo_all[2 * r + i], preferred_element_type=jnp.float32)
+        rest = resid[part, at_multiple(i * half_chunk, half_chunk, half_chunk)].astype(jnp.float32)
+        result(home_y, j, i)[...] = (rest + made).astype(jnp.bfloat16)
+        tp_move(0, j, i).start()
+        tp_move(1, j, i).start()
+
+    resid_copy.wait()
     for j in range(per):
-        make_mask(j)
-    attend_half(0, 0)
-    pl.when(late)(lambda: out_pass(0))
-    pl.when(jnp.logical_not(second_entry))(lambda: out_across(0))
-    attend_half(1, 1)
-    send_relay(A0)
-    pl.when(has_prev)(lambda: halo(1).wait_recv())
-    attend_half(1, 0)
-    pl.when(late)(lambda: out_pass(1))
-    out_across(1)
-    send_relay(A1)
-    pl.when(late)(lambda: out_pass(2))
-    out_across(2)
-    pl.when(late)(lambda: out_pass(3))
-    out_across(3)
-
-    for ch in (A0, A1):
         for d in range(nz):
-            pass_mine(ch, d)
-    for ch in (A0, A1):
-        for d in range(nz):
-            pass_theirs(ch, d)
-
-    half_chunk = chunk // 2
-
-    def store(which, i):
-        return pltpu.make_async_copy(
-            done.at[which, i], out_ref.at[:, at_multiple(which * chunk + i * half_chunk, half_chunk, half_chunk)],
-            store_sem.at[which, i],
-        )
-
-    def tp_move(way, i):
-        which, target = ((home_y, t_y), (home_y, t_core), (home, t_core))[way]
-        ref = done.at[which, i]
-        return remote(ref, ref, tp_send.at[way, i], tp_recv.at[way, i], tp=target)
-
-    def out_project(i):
-        made = jnp.zeros((rows, half_chunk), jnp.float32)
-        for r in range(n_tp):
-            made = made + jnp.dot(att_all[r], wo_all[2 * r + i], preferred_element_type=jnp.float32)
-        part = at_multiple(i * half_chunk, half_chunk, half_chunk)
-        done[home_y, i] = (resid[:, part].astype(jnp.float32) + made).astype(jnp.bfloat16)
-        tp_move(0, i).start()
-        tp_move(1, i).start()
-        store(home_y, i).start()
-
-    resid_copy.wait()
-    out_project(x)
+            pass_theirs(A0 + j, d)
+        out_project(j, x)
     for r in range(n_tp):
         across_in(OUT, r).wait_recv()
-    out_project(1 - x)
-    for i in (x, 1 - x):
-        tp_move(0, i).wait_recv()
-        tp_move(2, i).start()
-        store(home, i).start()
-    for i in (x, 1 - x):
-        tp_move(1, i).wait_recv()
-        store(plane_of(t_far), i).start()
-    for i in (x, 1 - x):
-        tp_move(2, i).wait_recv()
-        store(plane_of(t_core), i).start()
-    for which in range(n_tp):
-        for i in range(2):
-            store(which, i).wait()
+    for j in range(per):
+        out_project(j, 1 - x)
+    quarters = [(j, i) for i in (x, 1 - x) for j in range(per)]
+    for q in quarters:
+        tp_move(0, *q).wait_recv()
+        tp_move(2, *q).start()
+    for q in quarters:
+        tp_move(1, *q).wait_recv()
+        tp_move(2, *q).wait_recv()
 
     for ch in range(4):
         drain(ch)
@@ -757,13 +782,14 @@
 
     @pl.when(second_entry & inner)
     def _():
-        for r in range(pieces // 2, pieces):
-            aid_send_on(r).wait_send()
-
-    @pl.when(first_entry & inner)
-    def _():
-        for r in range(n_tp // 2, n_tp):
-            wo_aid_send_on(r).wait_send()
+        for i in range(4):
+            aid_move(i).wait_send()
+
+    @pl.when(aide)
+    def _():
+        for r in range(1, n_tp):
+            wo_aid_move(r).wait_send()
+
 
     @pl.when(first_entry)
     def _():
@@ -775,8 +801,8 @@
         for i in range(pairs + 1):
             halo(i).wait_send()
     for way in range(3):
-        for i in range(2):
-            tp_move(way, i).wait_send()
+        for q in quarters:
+            tp_move(way, *q).wait_send()
 
 
 def body_one(n_sp, n_tp, tokens, documents, norm_gain, w_query, w_key, w_value, w_out, rel_bias):
@@ -794,17 +820,17 @@
     q_rows, span = 2 * SEG, (LEFT + 2) * SEG
     return pl.pallas_call(
         functools.partial(layer_kernel, n_sp, n_tp),
-        out_shape=jax.ShapeDtypeStruct((rows, width), bf),
+        out_shape=pltpu.VMEM((rows, width), bf),
         in_specs=[hbm] * 8,
-        out_specs=hbm,
+        out_specs=pl.BlockSpec(memory_space=pltpu.VMEM),
         scratch_shapes=[
             pltpu.VMEM((2, pairs, depth, 3 * lanes), bf),
             pltpu.VMEM((pairs, depth, 3 * lanes), bf),
             pltpu.VMEM((pairs, n_sp * depth, 3 * lanes), bf),
             pltpu.VMEM((n_sp, cols, out_cols), bf),
             pltpu.VMEM((2, rows, width), bf),
-            pltpu.VMEM((rows // 2, width), bf),
-            pltpu.VMEM((n_tp // 2, cols, out_cols), bf),
+            pltpu.VMEM((4 * rows // (2 * n_tp), width), bf),
+            pltpu.VMEM((n_tp - 1, cols, out_cols), bf),
             pltpu.VMEM((rows, chunk), bf),
             pltpu.VMEM((2 * rows, width), bf),
             pltpu.VMEM((1, width), f32),
@@ -814,18 +840,17 @@
             pltpu.VMEM((pairs, 3 * rows, 2 * lanes), bf),
             pltpu.VMEM((1, 3 * rows), jnp.int32),
             pltpu.VMEM((2 * rows // q_rows, q_rows, span), f32),
-            pltpu.VMEM((pairs, 2, rows, lanes), bf),
-            pltpu.VMEM((pairs, rows, lanes), bf),
+            pltpu.VMEM((rows // q_rows, 2, q_rows, cols // 2), bf),
+            pltpu.VMEM((rows // q_rows, q_rows, cols // 2), bf),
             pltpu.VMEM((n_tp, rows, cols), bf),
-            pltpu.VMEM((n_tp, 2, rows, chunk // 2), bf),
             dma((2, pairs, 3)),
             dma((pairs, 3)),
             dma((n_tp,)),
-            dma((n_tp,)),
+            dma((2 * n_tp,)),
             dma(()),
-            dma((n_tp // 2,)),
-            dma((n_tp // 2,)),
-            dma((n_tp // 2,)),
+            dma((4,)),
+            dma((n_tp - 1,)),
+            dma((n_tp - 1,)),
             dma(()),
             dma((3,)),
             dma((3,)),
@@ -834,13 +859,12 @@
             dma((4,)),
             dma((4, 2, n_sp)),
             dma((4, n_sp)),
-            dma((2, 3, n_tp + 1)),
-            dma((2, 2, n_tp + 1)),
+            dma((2, 3, 2 * n_tp + 1)),
+            dma((2, 2, 2 * n_tp + 1)),
             dma((pairs + 1,)),
             dma((pairs + 1,)),
-            dma((3, 2)),
-            dma((3, 2)),
-            dma((n_tp, 2)),
+            dma((3, rows // q_rows, 2)),
+            dma((3, rows // q_rows, 2)),
         ],
         compiler_params=pltpu.CompilerParams(
             collective_id=0, has_side_effects=True, vmem_limit_bytes=60 * 1024 * 1024

time: 88.8 us -> 81.2 us (0.914)
  Pallas kernels: 85.2 us -> 79.2 us
  local copies, waits for them, and re-layouts: 2.3 us -> 0.97 us
    pallas_call x1, Pallas kernels: 85.2 us -> 79.2 us  [body_one(): pl.pallas_call(functools.partial(layer_kernel, n_sp, n_tp), out_shape=plt...]
    unnamed x1, local copies, waits for them, and re-layouts: 2.3 us -> 0.97 us
where the time goes in v3:
time: 81.2 us; the launch traced here: 80.2 us
  Pallas kernels  79.2 us (98%)
  local copies, waits for them, and re-layouts  0.97 us (1%)
    pallas_call x1, Pallas kernels, body_one(): pl.pallas_call(functools.partial(layer_kernel, n_sp, n_tp), out_shape=plt...  79.2 us

profile of v3, /device:TPU:0, one launch (start us, length us, event | category | flops | bytes accessed | tf_op | source)
XLA Modules:
  0.0 80.2 jit_solution(6373040146213420912)
XLA Ops:
  0.0 79.2 %shard_map.82 = bf16[256,2048]{1,0:T(8,128)(2,1)S(1)} custom-call(s32[1,256]{1,0:T(1,128)} %bitcast.11, f32[1,2048]{1,0:T(1,128)} %gain_in.1, f32[8,257]{1,0:T(8,128)} %bitcast.10, bf16[256,2048]{1,0:T(8,128)(2,1)} %x_in.1, bf16[256,512]{1,0:T(8,128)(2,1)} %bitcast.7, bf16[256,512]{1,0:T(8,128)(2,1)} %bitcast.8, bf16[256,512]{1,0:T(8,128)(2,1)} %bitcast.9, ...), custom_call_target="tpu_custom_call" | custom-call | tf_op jit(solution)/shard_map/pallas_call | solution.py:821
  79.2 1.0 %copy.10 = bf16[256,2048]{1,0:T(8,128)(2,1)} copy(bf16[256,2048]{1,0:T(8,128)(2,1)S(1)} %shard_map.82) | data formatting | bytes 2097152

commit v4 on v3

--- a/solution.py
+++ b/solution.py
@@ -137,7 +137,7 @@
     w_own, w_relay, w_all, wo_all, tok, aid, wo_aid, resid, normed, gain, table, bias, q_buf, kv_all, docs_all, mask,
     att_own, att_relay, att_all,
     own_sem, loc_sem, out_sem, tok_sem, aid_sem, aid_send, wo_aid_sem, wo_aid_send, res_sem, small_sem, line_send, line_recv, hop_send, relay_recv, rep_send, rep_recv,
-    cast_send, cast_recv, halo_send, halo_recv, tp_send, tp_recv,
+    cast_send, cast_recv, across_recv, halo_send, halo_recv, tp_send, tp_recv,
 ):
     rows, width = tok.shape[1:]
     depth, cols = wk_in.shape
@@ -148,6 +148,7 @@
     chunk = width // n_tp
     nz = n_sp // 2
     pieces = 2 * n_tp
+    aids = n_tp
     piece = rows // pieces
     s = lax.axis_index("sp")
     t = lax.axis_index("tp")
@@ -178,18 +179,16 @@
     def own_copy(i, p, kind):
         which = x if i == 0 else 1 - x
         return pltpu.make_async_copy(
-            own_in[kind].at[:, weight_cols(which, p)], w_own.at[i, p, :, kind_cols(kind)], own_sem.at[i, p, kind]
+            own_in[kind].at[:, weight_cols(which, p)], w_own.at[i, p, :, kind_cols(kind)], own_sem.at[i, p]
         )
 
     def local_copy(p, kind):
         return pltpu.make_async_copy(
             own_in[kind].at[:, weight_cols(x, p)],
-            w_all.at[p, at_multiple(s * depth, depth, depth), kind_cols(kind)], loc_sem.at[p, kind],
+            w_all.at[p, at_multiple(s * depth, depth, depth), kind_cols(kind)], loc_sem.at[p],
         )
 
-    def tok_copy(r):
-        part = pl.ds(r * piece, piece)
-        return pltpu.make_async_copy(x_in.at[part, :], tok.at[x, part, :], tok_sem.at[r])
+    tok_copy = pltpu.make_async_copy(x_in, tok.at[x], tok_sem)
 
     def out_copy(r):
         return pltpu.make_async_copy(wo_in.at[pl.ds(r * cols, cols), :], wo_all.at[2 * r + x], out_sem.at[r])
@@ -204,8 +203,7 @@
     @pl.when(first_entry)
     def _():
         doc_copy.start()
-        for r in range(pieces):
-            tok_copy(r).start()
+        tok_copy.start()
         table_copy.start()
 
     for p in range(pairs):
@@ -274,10 +272,10 @@
         return remote(relay_ref(ch), slot(ch, mate), hop_send.at[ch, 2], rep_recv.at[ch, mate], sp=2 * home_y + x)
 
     def to_y(ch, block):
-        return remote(slot(ch, block), slot(ch, block), rep_send.at[ch, 0, block], rep_recv.at[ch, block], tp=t_y)
+        return remote(slot(ch, block), slot(ch, block), rep_send.at[ch, 0], rep_recv.at[ch, block], tp=t_y)
 
     def to_core(ch, block):
-        return remote(slot(ch, block), slot(ch, block), rep_send.at[ch, 1, block], rep_recv.at[ch, block], tp=t_core)
+        return remote(slot(ch, block), slot(ch, block), rep_send.at[ch, 1], rep_recv.at[ch, block], tp=t_core)
 
     def send_cross(ch):
         pl.when(first_entry)(lambda: cross_in(ch).start())
@@ -308,8 +306,8 @@
                 if ch < A0:
                     @pl.when(first_entry)
                     def _():
-                        for kind in range(3):
-                            local_copy(ch - W0, kind).wait()
+                        wide = wk_in.at[:, pl.ds(0, 3 * lanes)]
+                        pltpu.make_async_copy(wide, slot(ch, s), loc_sem.at[ch - W0]).wait()
             else:
                 to_y(ch, block).wait_recv()
             to_y(ch, block).start()
@@ -343,10 +341,12 @@
 
         @pl.when(entry)
         def _():
-            for zz in range(nz):
-                to_y(ch, 2 * zz + x_mine).wait_send()
-                for i in range(2):
-                    to_core(ch, 2 * zz + i).wait_send()
+            if ch < A0:
+                some, every = w_all.at[ch - W0, pl.ds(0, nz * depth), :], w_all.at[ch - W0]
+            else:
+                some, every = att_all.at[0], att_all.at[pl.ds(0, 2)]
+            remote(some, some, rep_send.at[ch, 0], rep_recv.at[ch, 0], tp=t_y).wait_send()
+            remote(every, every, rep_send.at[ch, 1], rep_recv.at[ch, 0], tp=t_core).wait_send()
 
     def cast_ref(kind, which, r):
         if kind == OUT:
@@ -355,21 +355,33 @@
             return docs_all.at[:, at_multiple((1 + which) * rows, rows, rows)]
         return tok.at[which, pl.ds(r * piece, piece), :]
 
-    def move(kind, way, r, src=None):
+    def group_of(kind, r):
+        if kind == OUT:
+            return 3 if r == 0 else 4
+        return 2 if r == pieces else int(r >= pieces - aids)
+
+    def line_in(kind, r):
+        return cast_recv.at[r if kind == TOK else pieces + 1 + r]
+
+    def move(kind, way, r):
         ref = cast_ref(kind, x, r)
-        return remote(
-            ref if src is None else src, ref, cast_send.at[kind, way, r], cast_recv.at[kind, x, r],
-            sp=(s + 2, s - 2, mate)[way],
-        )
-
-    def across_in(kind, r):
-        ref = cast_ref(kind, 1 - x, r)
-        return remote(ref, ref, cast_send.at[kind, ACROSS, r], cast_recv.at[kind, 1 - x, r], sp=mate)
+        arrive = across_recv.at[(0, 0, 1, 2, 2)[group_of(kind, r)]] if way == ACROSS else line_in(kind, r)
+        return remote(ref, ref, cast_send.at[group_of(kind, r), way], arrive, sp=(s + 2, s - 2, mate)[way])
+
+    aid_rows = aids * piece
+    whole = (
+        tok.at[0, pl.ds(0, rows - aid_rows), :], tok.at[0, pl.ds(0, aid_rows), :], docs_all.at[:, pl.ds(0, rows)],
+        wo_all.at[0], wo_all.at[pl.ds(0, n_tp - 1)],
+    )
+
+    def across_all(i):
+        ref = (tok.at[1 - x], docs_all.at[:, at_multiple((2 - x) * rows, rows, rows)], wo_all.at[pl.ds(0, n_tp)])[i]
+        return remote(ref, ref, cast_send.at[0, ACROSS], across_recv.at[i], sp=mate)
 
     centers = (home, home_y)
 
     def aided(kind, r):
-        return pieces - 4 <= r < pieces if kind == TOK else r > 0
+        return pieces - aids <= r < pieces if kind == TOK else r > 0
 
     def goes(kind, way, r):
         ok = (z >= centers[kind]) & has_up if way == UP else (z <= centers[kind]) & has_down
@@ -379,32 +391,35 @@
         return ok
 
     def aid_move(i):
-        r = pieces - 4 + i
+        r = pieces - aids + i
         return remote(
-            aid.at[pl.ds(i * piece, piece), :], cast_ref(TOK, x, r), aid_send.at[i], cast_recv.at[TOK, x, r],
+            aid.at[pl.ds(i * piece, piece), :], cast_ref(TOK, x, r), aid_send, line_in(TOK, r),
             sp=s + 2 - 4 * (1 - z // (nz // 2)), tp=t_y,
         )
 
     def wo_aid_move(r):
         return remote(
-            wo_aid.at[r - 1], cast_ref(OUT, x, r), wo_aid_send.at[r - 1], cast_recv.at[OUT, x, r],
+            wo_aid.at[r - 1], cast_ref(OUT, x, r), wo_aid_send.at[r - 1], line_in(OUT, r),
             sp=s + 2 - 4 * (1 - z // (nz // 2)), tp=t_core,
         )
 
-    def cast_along(kind, r, src=None):
+    def cast_along(kind, r):
         for way in (UP, DOWN):
-            pl.when(goes(kind, way, r))(lambda: move(kind, way, r, src).start())
-
-    def cast_send_on(kind, r, src=None):
-        cast_along(kind, r, src)
-        move(kind, ACROSS, r, src).start()
+            pl.when(goes(kind, way, r))(lambda: move(kind, way, r).start())
+
+    def cast_send_on(kind, r):
+        cast_along(kind, r)
+        move(kind, ACROSS, r).start()
 
     def cast_source(kind, r):
         if r == pieces and kind == TOK:
             doc_copy.wait()
             cast_send_on(kind, r)
             return
-        (tok_copy, out_copy)[kind](r).wait()
+        if kind == OUT:
+            out_copy(r).wait()
+        elif r == 0:
+            tok_copy.wait()
         cast_send_on(kind, r)
 
     def cast_forward(kind, r):
@@ -413,11 +428,14 @@
             move(kind, UP, r).wait_recv()
             cast_send_on(kind, r)
 
-    def cast_drain(kind, count):
-        for r in range(count):
+    def cast_drain():
+        for g, (kind, r) in enumerate(((TOK, 0), (TOK, pieces - 1), (TOK, pieces), (OUT, 0), (OUT, 1))):
+            def done(way):
+                remote(whole[g], whole[g], cast_send.at[g, way], line_in(kind, r), sp=mate).wait_send()
+
             for way in (UP, DOWN):
-                pl.when(goes(kind, way, r))(lambda: move(kind, way, r).wait_send())
-            move(kind, ACROSS, r).wait_send()
+                pl.when(goes(kind, way, r))(lambda: done(way))
+            done(ACROSS)
 
     line_targets = (t_core, t_y, t_far)
 
@@ -452,8 +470,8 @@
 
     for p in range(pairs):
         for i in (1, 0):
-            for kind in range(3):
-                own_copy(i, p, kind).wait()
+            wide = wk_in.at[:, pl.ds(0, 3 * lanes)]
+            pltpu.make_async_copy(wide, w_own.at[i, p], own_sem.at[i, p]).wait()
             (send_direct, send_cross)[i](W0 + p)
 
     @pl.when(first_entry)
@@ -490,7 +508,7 @@
         @pl.when(inner)
         def _():
             aid_copy.wait()
-            for i in range(4):
+            for i in range(aids):
                 aid_move(i).start()
 
         @pl.when(outer)
@@ -646,8 +664,8 @@
     middle = jnp.logical_not(entry) & inner
 
     pl.when(middle)(lambda: out_pass(1))
-    for r in range(pieces + 1):
-        across_in(TOK, r).wait_recv()
+    for i in range(2):
+        across_all(i).wait_recv()
     pl.when(has_next)(lambda: halo(pairs).start())
     normalize(1 - x)
     late = jnp.logical_not(second_entry) & outer
@@ -746,7 +764,7 @@
     def tp_move(way, j, i):
         which, target = ((home_y, t_y), (home_y, t_core), (home, t_core))[way]
         ref = result(which, j, i)
-        return remote(ref, ref, tp_send.at[way, j, i], tp_recv.at[way, j, i], tp=target)
+        return remote(ref, ref, tp_send.at[way], tp_recv.at[way, j, i], tp=target)
 
     def out_project(j, i):
         part = pl.ds(j * q_rows, q_rows)
@@ -763,8 +781,7 @@
         for d in range(nz):
             pass_theirs(A0 + j, d)
         out_project(j, x)
-    for r in range(n_tp):
-        across_in(OUT, r).wait_recv()
+    across_all(2).wait_recv()
     for j in range(per):
         out_project(j, 1 - x)
     quarters = [(j, i) for i in (x, 1 - x) for j in range(per)]
@@ -777,13 +794,11 @@
 
     for ch in range(4):
         drain(ch)
-    cast_drain(TOK, pieces + 1)
-    cast_drain(OUT, n_tp)
+    cast_drain()
 
     @pl.when(second_entry & inner)
     def _():
-        for i in range(4):
-            aid_move(i).wait_send()
+        remote(aid, whole[1], aid_send, line_in(TOK, 0), tp=t_y).wait_send()
 
     @pl.when(aide)
     def _():
@@ -801,8 +816,8 @@
         for i in range(pairs + 1):
             halo(i).wait_send()
     for way in range(3):
-        for q in quarters:
-            tp_move(way, *q).wait_send()
+        ref = out_ref.at[:, pl.ds(0, chunk)]
+        remote(ref, ref, tp_send.at[way], tp_recv.at[way, 0, 0], tp=t_y).wait_send()
 
 
 def body_one(n_sp, n_tp, tokens, documents, norm_gain, w_query, w_key, w_value, w_out, rel_bias):
@@ -843,12 +858,12 @@
             pltpu.VMEM((rows // q_rows, 2, q_rows, cols // 2), bf),
             pltpu.VMEM((rows // q_rows, q_rows, cols // 2), bf),
             pltpu.VMEM((n_tp, rows, cols), bf),
-            dma((2, pairs, 3)),
-            dma((pairs, 3)),
+            dma((2, pairs)),
+            dma((pairs,)),
             dma((n_tp,)),
-            dma((2 * n_tp,)),
             dma(()),
-            dma((4,)),
+            dma(()),
+            dma(()),
             dma((n_tp - 1,)),
             dma((n_tp - 1,)),
             dma(()),
@@ -857,13 +872,14 @@
             dma(()),
             dma((4, 3)),
             dma((4,)),
-            dma((4, 2, n_sp)),
+            dma((4, 2)),
             dma((4, n_sp)),
-            dma((2, 3, 2 * n_tp + 1)),
-            dma((2, 2, 2 * n_tp + 1)),
+            dma((5, 3)),
+            dma((3 * n_tp + 1,)),
+            dma((3,)),
             dma((pairs + 1,)),
             dma((pairs + 1,)),
-            dma((3, rows // q_rows, 2)),
+            dma((3,)),
             dma((3, rows // q_rows, 2)),
         ],
         compiler_params=pltpu.CompilerParams(

time: 81.2 us -> 79.9 us (0.984)
  Pallas kernels: 79.2 us -> 77.8 us
    pallas_call x1, Pallas kernels: 79.2 us -> 77.8 us  [body_one(): pl.pallas_call(functools.partial(layer_kernel, n_sp, n_tp), out_shape=plt...]
where the time goes in v4:
time: 79.9 us; the launch traced here: 78.8 us
  Pallas kernels  77.8 us (97%)
  local copies, waits for them, and re-layouts  0.97 us (1%)
    pallas_call x1, Pallas kernels, body_one(): pl.pallas_call(functools.partial(layer_kernel, n_sp, n_tp), out_shape=plt...  77.8 us

profile of v4, /device:TPU:0, one launch (start us, length us, event | category | flops | bytes accessed | tf_op | source)
XLA Modules:
  0.0 78.8 jit_solution(11591713679573856254)
XLA Ops:
  0.0 77.8 %shard_map.82 = bf16[256,2048]{1,0:T(8,128)(2,1)S(1)} custom-call(s32[1,256]{1,0:T(1,128)} %bitcast.11, f32[1,2048]{1,0:T(1,128)} %gain_in.1, f32[8,257]{1,0:T(8,128)} %bitcast.10, bf16[256,2048]{1,0:T(8,128)(2,1)} %x_in.1, bf16[256,512]{1,0:T(8,128)(2,1)} %bitcast.7, bf16[256,512]{1,0:T(8,128)(2,1)} %bitcast.8, bf16[256,512]{1,0:T(8,128)(2,1)} %bitcast.9, ...), custom_call_target="tpu_custom_call" | custom-call | tf_op jit(solution)/shard_map/pallas_call | solution.py:836
  77.8 1.0 %copy.10 = bf16[256,2048]{1,0:T(8,128)(2,1)} copy(bf16[256,2048]{1,0:T(8,128)(2,1)S(1)} %shard_map.82) | data formatting | bytes 2097152

commit v5 on v4

--- a/solution.py
+++ b/solution.py
@@ -477,7 +477,12 @@
     @pl.when(first_entry)
     def _():
         for r in (pieces,) + tuple(range(pieces)):
-            cast_source(TOK, r)
+            if r in (2, 3):
+                pl.when((z <= home) & has_up & (outer | lower))(lambda: move(TOK, UP, r).start())
+                pl.when((z >= home) & has_down & (outer | jnp.logical_not(lower)))(lambda: move(TOK, DOWN, r).start())
+                move(TOK, ACROSS, r).start()
+            else:
+                cast_source(TOK, r)
         table_copy.wait()
         for i in range(3):
             line_copy(i).start()
@@ -539,6 +544,13 @@
         pass_mine(W1, 0)
         send_relay(W0)
         send_relay(W1)
+
+        @pl.when(inner)
+        def _():
+            for r in (2, 3):
+                pl.when(lower)(lambda: move(TOK, DOWN, r).start())
+                pl.when(jnp.logical_not(lower))(lambda: move(TOK, UP, r).start())
+
         for ch in (W0, W1):
             for d in range(1, nz):
                 pass_mine(ch, d)

time: 79.9 us -> 90.8 us (1.14)
  Pallas kernels: 77.8 us -> 89.4 us
    pallas_call x1, Pallas kernels: 77.8 us -> 89.4 us  [body_one(): pl.pallas_call(functools.partial(layer_kernel, n_sp, n_tp), out_shape=plt...]
where the time goes in v5:
time: 90.8 us; the launch traced here: 90.4 us
  Pallas kernels  89.4 us (98%)
  local copies, waits for them, and re-layouts  0.97 us (1%)
    pallas_call x1, Pallas kernels, body_one(): pl.pallas_call(functools.partial(layer_kernel, n_sp, n_tp), out_shape=plt...  89.4 us

profile of v5, /device:TPU:0, one launch (start us, length us, event | category | flops | bytes accessed | tf_op | source)
XLA Modules:
  0.0 90.4 jit_solution(4801725969267794253)
XLA Ops:
  0.0 89.4 %shard_map.82 = bf16[256,2048]{1,0:T(8,128)(2,1)S(1)} custom-call(s32[1,256]{1,0:T(1,128)} %bitcast.11, f32[1,2048]{1,0:T(1,128)} %gain_in.1, f32[8,257]{1,0:T(8,128)} %bitcast.10, bf16[256,2048]{1,0:T(8,128)(2,1)} %x_in.1, bf16[256,512]{1,0:T(8,128)(2,1)} %bitcast.7, bf16[256,512]{1,0:T(8,128)(2,1)} %bitcast.8, bf16[256,512]{1,0:T(8,128)(2,1)} %bitcast.9, ...), custom_call_target="tpu_custom_call" | custom-call | tf_op jit(solution)/shard_map/pallas_call | solution.py:848
  89.4 1.0 %copy.10 = bf16[256,2048]{1,0:T(8,128)(2,1)} copy(bf16[256,2048]{1,0:T(8,128)(2,1)S(1)} %shard_map.82) | data formatting | bytes 2097152
